TPU v7x, 32 devices: a whole 2x2x4 slice. The times are simulated.
32 devices in a mesh: grp: 2 (over x), ep: 16 (over z, y, core).
Axes of the slice: x: 2, y: 2, z: 4, core: 2. Of those that a mesh axis runs over, the one named last changes fastest.
Arguments:
- tokens: bfloat16 [8192, 2048], P(('grp', 'ep')), parts along dimension 0, may hold values from -6 to 6
- norm_gain: float32 [2048], replicated, may hold values from 0.1 to 1.9
- expert_ids: int32 [8192, 2], P(('grp', 'ep')), parts along dimension 0, may hold values from 0 to 15, all different within a row; in each aligned block of 256 rows (0 to 255, 256 to 511, ...) at most 64 rows name the same one
- gate_weights: float32 [8192, 2], P(('grp', 'ep')), parts along dimension 0, may hold values from 0.1 to 1
- w_gate: bfloat16 [16, 2048, 1024], P('ep'), may hold values from -0.125 to 0.125
- w_up: bfloat16 [16, 2048, 1024], P('ep'), may hold values from -0.125 to 0.125
- w_down: bfloat16 [16, 1024, 2048], P('ep'), may hold values from -0.1875 to 0.1875
Outputs:
- mixed: bfloat16 [8192, 2048], P(('grp', 'ep')), parts along dimension 0
There are 2 independent parts, one for each index of `grp`. A program takes and returns all parts, laid end to end along the dimension named above; an argument that names none is the same for every part. Nothing has to cross between parts.
Inputs may be any that keep to these rules, and one draw needn't show every extreme that they name: `expert_ids`: A token's 2 experts are distinct. Within the rows of one device (aligned blocks of 256 tokens) no expert is named more than 64 times, and in some block one expert is named exactly 64 times.
All inputs are finite; a program needn't handle non-finite values.
Results may differ from a plain program's by a relative error of at most 0.0071.
Values may be sent and summed in bfloat16 or wider, within the bound.
A program may use at most 64 MiB of HBM per device.

v0:
```python
import functools
import jax
import jax.numpy as jnp
from jax import lax
from jax.experimental import pallas as pl
from jax.experimental.pallas import tpu as pltpu
from jax.sharding import PartitionSpec as P

SUB = 4
HALVES = 2


def kernel(n, cap, tok_ref, gain_ref, ids_ref, gw_ref, wg_ref, wu_ref, wd_ref, out_ref,
           wg, wu, wd, lines, places, outgoing, arrived, results, returned, hidden, acc,
           send1, recv1, send2, recv2, wsem,
           lsend, lrecv, psend, precv,
           relay, dense, landed, rsend, rrecv, dsend, drecv):
    zs = n // SUB
    me = lax.axis_index("ep")
    hi, lo = me // SUB, me % SUB
    tok, width = tok_ref.shape
    ff = wg.shape[1]
    rows = SUB * cap

    barrier = pltpu.get_barrier_semaphore()

    def greet(r, carry):
        pl.semaphore_signal(barrier, inc=1, device_id={"ep": (me + r) % n},
                            device_id_type=pl.DeviceIdType.MESH)
        return carry

    lax.fori_loop(1, n, greet, 0)
    w_copies = [
        pltpu.make_async_copy(wg_ref.at[0], wg, wsem.at[0]),
        pltpu.make_async_copy(wu_ref.at[0], wu, wsem.at[1]),
        pltpu.make_async_copy(wd_ref.at[0], wd, wsem.at[2]),
    ]
    for c in w_copies:
        c.start()

    ids = ids_ref[...]
    id0, id1 = ids[:, 0:1], ids[:, 1:2]
    lane = lax.broadcasted_iota(jnp.int32, (tok, 128), 1)
    chosen = jnp.where((id0 == lane) | (id1 == lane), 1.0, 0.0)
    t_row = lax.broadcasted_iota(jnp.int32, (tok, tok), 0)
    t_col = lax.broadcasted_iota(jnp.int32, (tok, tok), 1)
    earlier = jnp.where(t_col < t_row, 1.0, 0.0).astype(jnp.bfloat16)
    before = jnp.dot(earlier, chosen.astype(jnp.bfloat16), preferred_element_type=jnp.float32)
    slot0 = jnp.sum(jnp.where(id0 == lane, before, 0.0), axis=1, keepdims=True)
    slot1 = jnp.sum(jnp.where(id1 == lane, before, 0.0), axis=1, keepdims=True)
    dest0 = id0.astype(jnp.float32) * cap + slot0
    dest1 = id1.astype(jnp.float32) * cap + slot1
    gw = gw_ref[...]
    g0, g1 = gw[:, 0:1], gw[:, 1:2]
    both = jnp.where(lane == 0, dest0, jnp.where(
        lane == 1, dest1, jnp.where(lane == 2, g0, jnp.where(lane == 3, g1, 0.0))))
    turned = jnp.transpose(both)

    step = 32

    def norm(i, carry):
        at = pl.ds(pl.multiple_of(i * step, step), step)
        v = tok_ref[at, :].astype(jnp.float32)
        scale = lax.rsqrt(jnp.mean(v * v, -1, keepdims=True) + 1e-06)
        lines[hi, at, :] = (v * scale * gain_ref[...]).astype(jnp.bfloat16)
        return carry

    lax.fori_loop(0, tok // step, norm, 0)

    def wait_all(copies):
        for c in copies:
            c.wait_recv()

    def line_copies(block, way):
        to = (hi + 2 * way - 1 + zs) % zs * SUB + lo
        return [
            pltpu.make_async_remote_copy(
                src_ref=buf.at[block], dst_ref=buf.at[block],
                send_sem=sends.at[way * zs + block], recv_sem=recvs.at[block],
                device_id={"ep": to}, device_id_type=pl.DeviceIdType.MESH)
            for buf, sends, recvs in ((places, psend, precv), (lines, lsend, lrecv))
        ]

    def pass_on(block, way):
        for c in line_copies(block, way):
            c.start()

    def slot_rows(j, dl):
        return pl.ds(pl.multiple_of(j * rows + dl * cap, cap), cap)

    def chunk_rows(j):
        return pl.ds(pl.multiple_of(j * rows, rows), rows)

    def out_copy(j, dl):
        at = slot_rows(j, dl)
        return pltpu.make_async_remote_copy(
            src_ref=outgoing.at[at, :], dst_ref=arrived.at[at, :],
            send_sem=send1.at[j * SUB + dl], recv_sem=recv1.at[j * SUB + dl],
            device_id={"ep": hi * SUB + (lo + dl) % SUB}, device_id_type=pl.DeviceIdType.MESH)

    def back_copy(j, dl):
        return pltpu.make_async_remote_copy(
            src_ref=results.at[slot_rows(j, dl), :], dst_ref=returned.at[slot_rows(hi, dl), :],
            send_sem=send2.at[j * SUB + dl], recv_sem=recv2.at[hi * SUB + dl],
            device_id={"ep": j * SUB + (lo - dl + SUB) % SUB}, device_id_type=pl.DeviceIdType.MESH)

    def back_arrival(j, dl):
        at = slot_rows(j, dl)
        return pltpu.make_async_remote_copy(
            src_ref=results.at[at, :], dst_ref=returned.at[at, :],
            send_sem=send2.at[j * SUB + dl], recv_sem=recv2.at[j * SUB + dl],
            device_id={"ep": j * SUB + (lo + dl) % SUB}, device_id_type=pl.DeviceIdType.MESH)

    def pack(j):
        r = lax.broadcasted_iota(jnp.int32, (rows, tok), 0)
        dl, s = r // cap, r % cap
        index = ((hi * SUB + (lo + dl) % SUB) * cap + s).astype(jnp.float32)
        where = places[j]
        pick = jnp.where((index == where[0:1, :]) | (index == where[1:2, :]), 1.0, 0.0)
        outgoing[chunk_rows(j), :] = jnp.dot(
            pick.astype(jnp.bfloat16), lines[j], preferred_element_type=jnp.float32
        ).astype(jnp.bfloat16)
        for dl in range(1, SUB):
            out_copy(j, dl).start()
        arrived[slot_rows(j, 0), :] = outgoing[slot_rows(j, 0), :]

    upper = hi // (zs - 2)
    meet = upper * (zs - 2) + (1 - upper)
    part = upper * (hi - (zs - 2)) + (1 - upper) * (1 - hi)
    half = width // HALVES

    def direct(plane, block):
        return jnp.logical_not(((plane >= zs - 2) & (block < zs - 2)) | ((plane <= 1) & (block > 1)))

    def relay_copy(j, dl, h):
        at = j - 2 * (1 - upper)
        cols = pl.ds(h * half, half)
        return pltpu.make_async_remote_copy(
            src_ref=results.at[slot_rows(j, dl), cols],
            dst_ref=relay.at[part, slot_rows(at, dl), cols],
            send_sem=rsend.at[(at * SUB + dl) * HALVES + h],
            recv_sem=rrecv.at[((part * (zs - 2) + at) * SUB + dl) * HALVES + h],
            device_id={"ep": meet * SUB + (lo - dl + SUB) % SUB},
            device_id_type=pl.DeviceIdType.MESH)

    def relay_arrival(p, at, dl, h):
        cols = pl.ds(h * half, half)
        sem = ((p * (zs - 2) + at) * SUB + dl) * HALVES + h
        return pltpu.make_async_remote_copy(
            src_ref=relay.at[p, slot_rows(at, dl), cols],
            dst_ref=relay.at[p, slot_rows(at, dl), cols],
            send_sem=rsend.at[(at * SUB + dl) * HALVES + h], recv_sem=rrecv.at[sem],
            device_id={"ep": meet * SUB + (lo + 1) % SUB}, device_id_type=pl.DeviceIdType.MESH)

    def dense_copy(at, h):
        cols = pl.ds(h * half, half)
        return pltpu.make_async_remote_copy(
            src_ref=dense.at[at, :, cols], dst_ref=landed.at[upper, :, cols],
            send_sem=dsend.at[at * HALVES + h], recv_sem=drecv.at[upper * HALVES + h],
            device_id={"ep": (at + 2 * (1 - upper)) * SUB + lo},
            device_id_type=pl.DeviceIdType.MESH)

    def dense_arrival(end, h):
        cols = pl.ds(h * half, half)
        return pltpu.make_async_remote_copy(
            src_ref=landed.at[end, :, cols], dst_ref=landed.at[end, :, cols],
            send_sem=dsend.at[h], recv_sem=drecv.at[end * HALVES + h],
            device_id={"ep": (me + 1) % n}, device_id_type=pl.DeviceIdType.MESH)

    ftile = min(ff, 256)
    dtile = min(width, 256)

    def experts(j):
        at = chunk_rows(j)
        for dl in range(1, SUB):
            out_copy(j, dl).wait_recv()

        def up(f, carry):
            cols = pl.ds(pl.multiple_of(f * ftile, ftile), ftile)
            x = arrived[at, :]
            g = jnp.dot(x, wg[:, cols], preferred_element_type=jnp.float32)
            u = jnp.dot(x, wu[:, cols], preferred_element_type=jnp.float32)
            hidden[:, cols] = (g / (1.0 + jnp.exp(-g)) * u).astype(jnp.bfloat16)
            return carry

        lax.fori_loop(0, ff // ftile, up, 0)

        def down(d, carry):
            cols = pl.ds(pl.multiple_of(d * dtile, dtile), dtile)
            results[at, cols] = jnp.dot(
                hidden[...], wd[:, cols], preferred_element_type=jnp.float32).astype(jnp.bfloat16)
            return carry

        lax.fori_loop(0, width // dtile, down, 0)

        @pl.when(direct(hi, j))
        def _():
            for dl in range(1, SUB):
                back_copy(j, dl).start()

        @pl.when(j == hi)
        def _():
            returned[slot_rows(hi, 0), :] = results[slot_rows(hi, 0), :]

        @pl.when((j != hi) & direct(hi, j))
        def _():
            back_copy(j, 0).start()

        @pl.when(jnp.logical_not(direct(hi, j)))
        def _():
            for h in range(HALVES):
                for dl in range(1, SUB):
                    relay_copy(j, dl, h).start()

                @pl.when(hi != meet)
                def _():
                    relay_copy(j, 0, h).start()

            @pl.when(hi == meet)
            def _():
                relay[0, slot_rows(j - 2 * (1 - upper), 0), :] = results[slot_rows(j, 0), :]

    def both_sides(s, act):
        @pl.when(hi - s >= 0)
        def _():
            act((hi - s + zs) % zs, 1)

        @pl.when(hi + s < zs)
        def _():
            act((hi + s) % zs, 0)

    def forward(block, way):
        @pl.when(hi < zs - 1 if way else hi > 0)
        def _():
            pass_on(block, way)

    def line_arrival(block, way):
        wait_all(line_copies(block, way))

    where = lax.broadcasted_iota(jnp.int32, (8, tok), 0)
    places[hi] = jnp.where(
        where == 0, turned[0:1, :], jnp.where(
            where == 1, turned[1:2, :], jnp.where(where == 2, turned[2:3, :], turned[3:4, :])))
    pl.semaphore_wait(barrier, n - 1)
    forward(hi, 1)
    forward(hi, 0)
    pack(hi)
    for c in w_copies:
        c.wait()

    experts(hi)

    side = 1 - 2 * (hi // ((zs + 1) // 2))

    def along(s, act):
        block = hi + side * s

        @pl.when((block >= 0) & (block < zs))
        def _():
            act((block + zs) % zs)

    def step_in(s, carry):
        def take(block, way):
            line_arrival(block, way)
            forward(block, way)

        both_sides(s, take)
        along(s, pack)
        along(-s, pack)

        @pl.when(s > 1)
        def _():
            along(1 - s, experts)

        along(s, experts)
        return carry

    lax.fori_loop(1, zs, step_in, 0)
    along(1 - zs, experts)

    def share(p, at, cols):
        block_places = places[at + 2 * (1 - upper)]
        r = lax.broadcasted_iota(jnp.int32, (rows, tok), 0)
        dl, s = r // cap, r % cap
        plane = upper * (zs - 2 + p) + (1 - upper) * (1 - p)
        index = ((plane * SUB + (lo + dl) % SUB) * cap + s).astype(jnp.float32)
        weight = (jnp.where(index == block_places[0:1, :], block_places[2:3, :], 0.0)
                  + jnp.where(index == block_places[1:2, :], block_places[3:4, :], 0.0))
        high = weight.astype(jnp.bfloat16)
        low = (weight - high.astype(jnp.float32)).astype(jnp.bfloat16)
        block = relay[p, chunk_rows(at), cols]
        dims = (((0,), (0,)), ((), ()))
        return (lax.dot_general(high, block, dims, preferred_element_type=jnp.float32)
                + lax.dot_general(low, block, dims, preferred_element_type=jnp.float32))

    @pl.when(hi == meet)
    def _():
        def meeting(t, carry):
            at = upper * (zs - 3 - t) + (1 - upper) * t
            for h in range(HALVES):
                cols = pl.ds(h * half, half)
                wait_all([relay_arrival(0, at, dl, h) for dl in range(1, SUB)])
                wait_all([relay_arrival(1, at, dl, h) for dl in range(SUB)])
                dense[at, :, cols] = (share(0, at, cols) + share(1, at, cols)).astype(jnp.bfloat16)
                dense_copy(at, h).start()
            return carry

        lax.fori_loop(0, zs - 2, meeting, 0)

    def gather(j):
        c = lax.broadcasted_iota(jnp.int32, (tok, rows), 1)
        dl, s = c // cap, c % cap
        index = ((j * SUB + (lo + dl) % SUB) * cap + s).astype(jnp.float32)
        weight = jnp.where(index == dest0, g0, 0.0) + jnp.where(index == dest1, g1, 0.0)
        high = weight.astype(jnp.bfloat16)
        low = (weight - high.astype(jnp.float32)).astype(jnp.bfloat16)
        block = returned[chunk_rows(j), :]
        return (jnp.dot(high, block, preferred_element_type=jnp.float32)
                + jnp.dot(low, block, preferred_element_type=jnp.float32))

    wait_all([back_arrival(hi, dl) for dl in range(1, SUB)])
    acc[...] = gather(hi)

    def combine(s, carry):
        def add(block, way):
            @pl.when(direct(block, hi))
            def _():
                wait_all([back_arrival(block, dl) for dl in range(SUB)])
                acc[...] += gather(block)

        both_sides(s, add)
        return carry

    lax.fori_loop(1, zs, combine, 0)
    for end in (0, 1):
        @pl.when(hi < zs - 2 if end else hi > 1)
        def _():
            for h in range(HALVES):
                cols = pl.ds(h * half, half)
                dense_arrival(end, h).wait_recv()
                acc[:, cols] += landed[end, :, cols].astype(jnp.float32)
    out_ref[...] = acc[...].astype(out_ref.dtype)

    def finish(j, carry):
        for dl in range(1, SUB):
            out_copy(j, dl).wait_send()

        @pl.when(direct(hi, j))
        def _():
            for dl in range(1, SUB):
                back_copy(j, dl).wait_send()

        @pl.when((j != hi) & direct(hi, j))
        def _():
            back_copy(j, 0).wait_send()

        @pl.when(jnp.logical_not(direct(hi, j)))
        def _():
            for h in range(HALVES):
                for dl in range(1, SUB):
                    relay_copy(j, dl, h).wait_send()

                @pl.when(hi != meet)
                def _():
                    relay_copy(j, 0, h).wait_send()

                @pl.when(hi == meet)
                def _():
                    dense_copy(j - 2 * (1 - upper), h).wait_send()

        for way in (0, 1):
            @pl.when((hi < zs - 1) & (j <= hi) if way else (hi > 0) & (j >= hi))
            def _():
                for c in line_copies(j, way):
                    c.wait_send()

        return carry

    lax.fori_loop(0, zs, finish, 0)


def per_device(tokens, norm_gain, expert_ids, gate_weights, w_gate, w_up, w_down):
    n = lax.axis_size("ep")
    tok, width = tokens.shape
    top = expert_ids.shape[1]
    ff = w_gate.shape[2]
    cap = 2 * tok * top // n
    total = n * cap
    bf16 = jnp.bfloat16
    vmem = pl.BlockSpec(memory_space=pltpu.VMEM)
    hbm = pl.BlockSpec(memory_space=pl.ANY)
    return pl.pallas_call(
        functools.partial(kernel, n, cap),
        out_shape=jax.ShapeDtypeStruct((tok, width), bf16),
        in_specs=[vmem] * 4 + [hbm] * 3,
        out_specs=vmem,
        scratch_shapes=[
            pltpu.VMEM((width, ff), bf16),
            pltpu.VMEM((width, ff), bf16),
            pltpu.VMEM((ff, width), bf16),
            pltpu.VMEM((n // SUB, tok, width), bf16),
            pltpu.VMEM((n // SUB, 8, tok), jnp.float32),
            pltpu.VMEM((total, width), bf16),
            pltpu.VMEM((total, width), bf16),
            pltpu.VMEM((total, width), bf16),
            pltpu.VMEM((total, width), bf16),
            pltpu.VMEM((SUB * cap, ff), bf16),
            pltpu.VMEM((tok, width), jnp.float32),
            pltpu.SemaphoreType.DMA((n,)),
            pltpu.SemaphoreType.DMA((n,)),
            pltpu.SemaphoreType.DMA((n,)),
            pltpu.SemaphoreType.DMA((n,)),
            pltpu.SemaphoreType.DMA((3,)),
            pltpu.SemaphoreType.DMA((2 * n // SUB,)),
            pltpu.SemaphoreType.DMA((n // SUB,)),
            pltpu.SemaphoreType.DMA((2 * n // SUB,)),
            pltpu.SemaphoreType.DMA((n // SUB,)),
            pltpu.VMEM((2, (n // SUB - 2) * SUB * cap, width), bf16),
            pltpu.VMEM((n // SUB - 2, tok, width), bf16),
            pltpu.VMEM((2, tok, width), bf16),
            pltpu.SemaphoreType.DMA(((n - 2 * SUB) * HALVES,)),
            pltpu.SemaphoreType.DMA((2 * (n - 2 * SUB) * HALVES,)),
            pltpu.SemaphoreType.DMA(((n // SUB - 2) * HALVES,)),
            pltpu.SemaphoreType.DMA((2 * HALVES,)),
        ],
        compiler_params=pltpu.CompilerParams(
            collective_id=0, has_side_effects=True, vmem_limit_bytes=62 * 1024 * 1024),
    )(tokens, norm_gain.reshape(1, width), expert_ids, gate_weights, w_gate, w_up, w_down)


def solution(mesh):
    return jax.shard_map(
        per_device,
        mesh=mesh,
        in_specs=(
            P(("grp", "ep"), None),
            P(),
            P(("grp", "ep"), None),
            P(("grp", "ep"), None),
            P("ep", None, None),
            P("ep", None, None),
            P("ep", None, None),
        ),
        out_specs=P(("grp", "ep"), None),
        check_vma=False,
    )
```

profile of v0, /device:TPU:1, one launch (start us, length us, event | category | flops | bytes accessed | tf_op | source)
XLA Modules:
  0.0 158.4 jit_solution(635317648594757041)
XLA Ops:
  0.0 1.5 copy.8.ids_ref
  1.5 1.5 copy.9.gw_ref
  2.9 153.2 %shard_map.73 = bf16[256,2048]{1,0:T(8,128)(2,1)} custom-call(bf16[256,2048]{1,0:T(8,128)(2,1)} %tok_ref.1, f32[1,2048]{1,0:T(1,128)} %bitcast.1, s32[256,2]{1,0:T(8,128)} %copy.8.ids_ref, f32[256,2]{1,0:T(8,128)} %copy.9.gw_ref, bf16[1,2048,1024]{2,1,0:T(8,128)(2,1)} %wg_ref.1, bf16[1,2048,1024]{2,1,0:T(8,128)(2,1)} %wu_ref.1, bf16[1,1024,2048]{2,1,0:T(8,128)(2,1)} %wd_ref.1), custom_call_target="tpu_custom_call" | custom-call | tf_op jit(solution)/shard_map/pallas_call | solution.py:392
  156.1 2.3 %copy.11 = bf16[256,2048]{1,0:T(8,128)(2,1)} copy(bf16[256,2048]{1,0:T(8,128)(2,1)} %shard_map.73) | data formatting | bytes 2097152
where the time goes:
time: 159 us; the launch traced here: 158 us
  Pallas kernels  153 us (96%)
  local copies, waits for them, and re-layouts  5.24 us (3%)
    pallas_call x1, Pallas kernels, per_device(): pl.pallas_call(functools.partial(kernel, n, cap), out_shape=jax.ShapeDtyp...  153 us
    unnamed x3, local copies, waits for them, and re-layouts  5.24 us

commit v1 on v0

v1 whole, which is shorter than its diff:
```python
import functools
import jax
import jax.numpy as jnp
from jax import lax
from jax.experimental import pallas as pl
from jax.experimental.pallas import tpu as pltpu
from jax.sharding import PartitionSpec as P

SUB = 4
KD = 4
KR = 4


def kernel(n, cap, tok_ref, gain_ref, ids_ref, gw_ref, wg_ref, wu_ref, wd_ref, out_ref,
           wg, wu, wd, lines, places, outgoing, arrived, results, returned, hidden, chain,
           pick, high, low,
           wsem, lsend, lrecv, psend, precv, dsend, drecv, bsend, brecv, csend, crecv):
    zs = n // SUB
    me = lax.axis_index("ep")
    hi, lo = me // SUB, me % SUB
    tok, width = tok_ref.shape
    ff = wg.shape[1]
    rows = SUB * cap
    dcols, rcols = width // KD, width // KR
    own = 2

    def peer(plane, part):
        return {"ep": plane * SUB + part}

    barrier = pltpu.get_barrier_semaphore()

    def greet(to):
        pl.semaphore_signal(barrier, inc=1, device_id=to, device_id_type=pl.DeviceIdType.MESH)

    for dl in range(1, SUB):
        greet(peer(hi, (lo + dl) % SUB))

    @pl.when(hi > 0)
    def _():
        greet(peer((hi + zs - 1) % zs, lo))

    @pl.when(hi < zs - 1)
    def _():
        greet(peer((hi + 1) % zs, lo))

    w_copies = [
        pltpu.make_async_copy(wg_ref.at[0], wg, wsem.at[0]),
        pltpu.make_async_copy(wu_ref.at[0], wu, wsem.at[1]),
        pltpu.make_async_copy(wd_ref.at[0], wd, wsem.at[2]),
    ]
    for c in w_copies:
        c.start()

    def remote(src, dst, send, recv, to):
        return pltpu.make_async_remote_copy(
            src_ref=src, dst_ref=dst, send_sem=send, recv_sem=recv,
            device_id=to, device_id_type=pl.DeviceIdType.MESH)

    def dcol(k):
        return pl.ds(pl.multiple_of(k * dcols, dcols), dcols)

    def rcol(k):
        return pl.ds(pl.multiple_of(k * rcols, rcols), rcols)

    def slot_rows(j, dl):
        return pl.ds(pl.multiple_of(j * rows + dl * cap, cap), cap)

    def block_rows(j):
        return pl.ds(pl.multiple_of(j * rows, rows), rows)

    def far_rows(j):
        return pl.ds(pl.multiple_of(j * rows + cap, cap), rows - cap)

    def onward(way):
        return (hi + 2 * way - 1 + zs) % zs

    def line_copy(block, k, way):
        part = lines.at[block, :, dcol(k)]
        return remote(part, part, lsend.at[way * zs + block], lrecv.at[block * KD + k],
                      peer(onward(way), lo))

    def place_copy(block, way):
        return remote(places.at[block], places.at[block], psend.at[way * zs + block],
                      precv.at[block], peer(onward(way), lo))

    def out_copy(j, dl, k):
        at = slot_rows(j, dl)
        return remote(outgoing.at[at, dcol(k)], arrived.at[at, dcol(k)],
                      dsend.at[j], drecv.at[j * KD + k], peer(hi, (lo + dl) % SUB))

    def out_arrival(j, k):
        at = arrived.at[far_rows(j), dcol(k)]
        return remote(at, at, dsend.at[j], drecv.at[j * KD + k], peer(hi, (lo + 1) % SUB))

    def back_copy(j, dl, k):
        at = slot_rows(j, dl)
        return remote(results.at[at, rcol(k)], returned.at[at, rcol(k)],
                      bsend.at[j], brecv.at[j * KR + k], peer(hi, (lo - dl + SUB) % SUB))

    def back_arrival(j, k):
        at = returned.at[far_rows(j), rcol(k)]
        return remote(at, at, bsend.at[j], brecv.at[j * KR + k], peer(hi, (lo + 1) % SUB))

    def chain_copy(way, j, k):
        part = chain.at[way * zs + j, :, rcol(k)]
        return remote(part, part, csend.at[way * zs + j], crecv.at[(way * zs + j) * KR + k],
                      peer(onward(way), lo))

    step = 32

    def norm(i, carry):
        at = pl.ds(pl.multiple_of(i * step, step), step)
        v = tok_ref[at, :].astype(jnp.float32)
        scale = lax.rsqrt(jnp.mean(v * v, -1, keepdims=True) + 1e-06)
        lines[hi, at, :] = (v * scale * gain_ref[...]).astype(jnp.bfloat16)
        return carry

    lax.fori_loop(0, tok // step, norm, 0)

    ends = jnp.where(hi == 0, 1, 0) + jnp.where(hi == zs - 1, 1, 0)
    pl.semaphore_wait(barrier, SUB + 1 - ends)

    def forward(way, act):
        @pl.when(jnp.where(way == 1, zs - 1 - hi, hi) > 0)
        def _():
            act(way)

    for way in (1, 0):
        forward(way, lambda w: line_copy(hi, 0, w).start())

    ids = ids_ref[...]
    id0, id1 = ids[:, 0:1], ids[:, 1:2]
    lane = lax.broadcasted_iota(jnp.int32, (tok, 128), 1)
    chosen = jnp.where((id0 == lane) | (id1 == lane), 1.0, 0.0)
    t_row = lax.broadcasted_iota(jnp.int32, (tok, tok), 0)
    t_col = lax.broadcasted_iota(jnp.int32, (tok, tok), 1)
    earlier = jnp.where(t_col < t_row, 1.0, 0.0).astype(jnp.bfloat16)
    before = jnp.dot(earlier, chosen.astype(jnp.bfloat16), preferred_element_type=jnp.float32)
    slot0 = jnp.sum(jnp.where(id0 == lane, before, 0.0), axis=1, keepdims=True)
    slot1 = jnp.sum(jnp.where(id1 == lane, before, 0.0), axis=1, keepdims=True)
    dest0 = id0.astype(jnp.float32) * cap + slot0
    dest1 = id1.astype(jnp.float32) * cap + slot1
    gw = gw_ref[...]
    g0, g1 = gw[:, 0:1], gw[:, 1:2]
    both = jnp.where(lane == 0, dest0, jnp.where(
        lane == 1, dest1, jnp.where(lane == 2, g0, jnp.where(lane == 3, g1, 0.0))))
    turned = jnp.transpose(both)
    where = lax.broadcasted_iota(jnp.int32, (8, tok), 0)
    places[hi] = jnp.where(
        where == 0, turned[0:1, :], jnp.where(
            where == 1, turned[1:2, :], jnp.where(where == 2, turned[2:3, :], turned[3:4, :])))

    def send_own(way):
        place_copy(hi, way).start()
        for k in range(1, KD):
            line_copy(hi, k, way).start()

    for way in (1, 0):
        forward(way, send_own)

    def row_index():
        r = lax.broadcasted_iota(jnp.int32, (rows, tok), 0)
        return ((hi * SUB + (lo + r // cap) % SUB) * cap + r % cap).astype(jnp.float32)

    def choose(j, at):
        index = row_index()
        w = places[j]
        pick[at] = jnp.where((index == w[0:1, :]) | (index == w[1:2, :]), 1.0, 0.0).astype(
            jnp.bfloat16)

    def pack(j, k, at):
        got = jnp.dot(pick[at], lines[j, :, dcol(k)],
                      preferred_element_type=jnp.float32).astype(jnp.bfloat16)
        outgoing[far_rows(j), dcol(k)] = got[cap:, :]
        for dl in range(1, SUB):
            out_copy(j, dl, k).start()
        arrived[slot_rows(j, 0), dcol(k)] = got[:cap, :]

    ftile = min(ff, 256)

    def experts(j):
        at = block_rows(j)

        def landed(k, carry):
            out_arrival(j, k).wait_recv()
            return carry

        lax.fori_loop(0, KD, landed, 0)

        def up(f, carry):
            cols = pl.ds(pl.multiple_of(f * ftile, ftile), ftile)
            x = arrived[at, :]
            g = jnp.dot(x, wg[:, cols], preferred_element_type=jnp.float32)
            u = jnp.dot(x, wu[:, cols], preferred_element_type=jnp.float32)
            hidden[:, cols] = (g / (1.0 + jnp.exp(-g)) * u).astype(jnp.bfloat16)
            return carry

        lax.fori_loop(0, ff // ftile, up, 0)

        def down(k, carry):
            got = jnp.dot(hidden[...], wd[:, rcol(k)],
                          preferred_element_type=jnp.float32).astype(jnp.bfloat16)
            results[far_rows(j), rcol(k)] = got[cap:, :]
            for dl in range(1, SUB):
                back_copy(j, dl, k).start()
            returned[slot_rows(j, 0), rcol(k)] = got[:cap, :]
            return carry

        lax.fori_loop(0, KR, down, 0)

    def weigh(j, at):
        index = row_index()
        w = places[j]
        weight = jnp.transpose(jnp.where(index == w[0:1, :], w[2:3, :], 0.0)
                               + jnp.where(index == w[1:2, :], w[3:4, :], 0.0))
        top = weight.astype(jnp.bfloat16)
        high[at] = top
        low[at] = (weight - top.astype(jnp.float32)).astype(jnp.bfloat16)

    def mix(j, k, at):
        block = returned[block_rows(j), rcol(k)]
        return (jnp.dot(high[at], block, preferred_element_type=jnp.float32)
                + jnp.dot(low[at], block, preferred_element_type=jnp.float32))

    choose(hi, own)

    def pack_own(k, carry):
        pack(hi, k, own)
        return carry

    lax.fori_loop(0, KD, pack_own, 0)
    for c in w_copies:
        c.wait()

    experts(hi)
    weigh(hi, own)

    first = hi // ((zs + 1) // 2)
    ways = (first, 1 - first)

    def arriving(s, act):
        for way in ways:
            block = hi + (1 - 2 * way) * s

            @pl.when((block >= 0) & (block < zs))
            def _():
                act((block + zs) % zs, way)

    def stage(s):
        def begin(block, way):
            place_copy(block, way).wait_recv()
            forward(way, lambda w: place_copy(block, w).start())
            choose(block, way)

        arriving(s, begin)

        def chunk(k, carry):
            def take(block, way):
                line_copy(block, k, way).wait_recv()
                forward(way, lambda w: line_copy(block, k, w).start())
                pack(block, k, way)

            arriving(s, take)
            return carry

        lax.fori_loop(0, KD, chunk, 0)
        arriving(s, lambda block, way: experts(block))

    def leaving(t, act):
        for way in (1, 0):
            j = way * t + (1 - way) * (zs - 1 - t)

            @pl.when(j > hi if way else j < hi)
            def _():
                act(j, way)

    def give(t):
        leaving(t, lambda j, way: weigh(j, way))

        def chunk(k, carry):
            def add(j, way):
                back_arrival(j, k).wait_recv()
                value = mix(j, k, way)
                at = way * zs + j

                @pl.when(hi > 0 if way else hi < zs - 1)
                def _():
                    chain_copy(way, j, k).wait_recv()
                    chain[at, :, rcol(k)] = (
                        value + chain[at, :, rcol(k)].astype(jnp.float32)).astype(jnp.bfloat16)

                @pl.when(hi == 0 if way else hi == zs - 1)
                def _():
                    chain[at, :, rcol(k)] = value.astype(jnp.bfloat16)

                chain_copy(way, j, k).start()

            leaving(t, add)
            return carry

        lax.fori_loop(0, KR, chunk, 0)

    def turn(s, carry):
        stage(s)
        give(s)
        return carry

    lax.fori_loop(1, zs, turn, 0)

    def final(k, carry):
        back_arrival(hi, k).wait_recv()
        value = mix(hi, k, own)

        @pl.when(hi == 0)
        def _():
            chain_copy(0, hi, k).wait_recv()
            out_ref[:, rcol(k)] = (
                value + chain[hi, :, rcol(k)].astype(jnp.float32)).astype(out_ref.dtype)

        @pl.when(hi == zs - 1)
        def _():
            chain_copy(1, hi, k).wait_recv()
            out_ref[:, rcol(k)] = (
                value + chain[zs + hi, :, rcol(k)].astype(jnp.float32)).astype(out_ref.dtype)

        @pl.when((hi > 0) & (hi < zs - 1))
        def _():
            chain_copy(0, hi, k).wait_recv()
            chain_copy(1, hi, k).wait_recv()
            out_ref[:, rcol(k)] = (
                value + chain[hi, :, rcol(k)].astype(jnp.float32)
                + chain[zs + hi, :, rcol(k)].astype(jnp.float32)).astype(out_ref.dtype)

        return carry

    lax.fori_loop(0, KR, final, 0)

    def finish(j, carry):
        at = far_rows(j)
        remote(outgoing.at[at, :], outgoing.at[at, :], dsend.at[j], drecv.at[0],
               peer(hi, (lo + 1) % SUB)).wait_send()
        remote(results.at[at, :], results.at[at, :], bsend.at[j], brecv.at[0],
               peer(hi, (lo + 1) % SUB)).wait_send()
        for way in (0, 1):
            to = peer(onward(way), lo)

            @pl.when((hi < zs - 1) & (j <= hi) if way else (hi > 0) & (j >= hi))
            def _():
                place_copy(j, way).wait_send()
                remote(lines.at[j], lines.at[j], lsend.at[way * zs + j], lrecv.at[0],
                       to).wait_send()

            @pl.when(j > hi if way else j < hi)
            def _():
                at = way * zs + j
                remote(chain.at[at], chain.at[at], csend.at[at], crecv.at[0], to).wait_send()

        return carry

    lax.fori_loop(0, zs, finish, 0)


def per_device(tokens, norm_gain, expert_ids, gate_weights, w_gate, w_up, w_down):
    n = lax.axis_size("ep")
    tok, width = tokens.shape
    top = expert_ids.shape[1]
    ff = w_gate.shape[2]
    cap = 2 * tok * top // n
    total = n * cap
    zs = n // SUB
    rows = SUB * cap
    bf16 = jnp.bfloat16
    dma = pltpu.SemaphoreType.DMA
    vmem = pl.BlockSpec(memory_space=pltpu.VMEM)
    hbm = pl.BlockSpec(memory_space=pl.ANY)
    return pl.pallas_call(
        functools.partial(kernel, n, cap),
        out_shape=jax.ShapeDtypeStruct((tok, width), bf16),
        in_specs=[vmem] * 4 + [hbm] * 3,
        out_specs=vmem,
        scratch_shapes=[
            pltpu.VMEM((width, ff), bf16),
            pltpu.VMEM((width, ff), bf16),
            pltpu.VMEM((ff, width), bf16),
            pltpu.VMEM((zs, tok, width), bf16),
            pltpu.VMEM((zs, 8, tok), jnp.float32),
            pltpu.VMEM((total, width), bf16),
            pltpu.VMEM((total, width), bf16),
            pltpu.VMEM((total, width), bf16),
            pltpu.VMEM((total, width), bf16),
            pltpu.VMEM((rows, ff), bf16),
            pltpu.VMEM((2 * zs, tok, width), bf16),
            pltpu.VMEM((3, rows, tok), bf16),
            pltpu.VMEM((3, tok, rows), bf16),
            pltpu.VMEM((3, tok, rows), bf16),
            dma((3,)),
            dma((2 * zs,)),
            dma((zs * KD,)),
            dma((2 * zs,)),
            dma((zs,)),
            dma((zs,)),
            dma((zs * KD,)),
            dma((zs,)),
            dma((zs * KR,)),
            dma((2 * zs,)),
            dma((2 * zs * KR,)),
        ],
        compiler_params=pltpu.CompilerParams(
            collective_id=0, has_side_effects=True, vmem_limit_bytes=62 * 1024 * 1024),
    )(tokens, norm_gain.reshape(1, width), expert_ids, gate_weights, w_gate, w_up, w_down)


def solution(mesh):
    return jax.shard_map(
        per_device,
        mesh=mesh,
        in_specs=(
            P(("grp", "ep"), None),
            P(),
            P(("grp", "ep"), None),
            P(("grp", "ep"), None),
            P("ep", None, None),
            P("ep", None, None),
            P("ep", None, None),
        ),
        out_specs=P(("grp", "ep"), None),
        check_vma=False,
    )
```

time: 159 us -> 186 us (1.17)
  the two profiles are of different devices: /device:TPU:1 before, /device:TPU:0 now
where the time goes in v1:
time: 186 us
  Pallas kernels  181 us (97%)
  local copies, waits for them, and re-layouts  5.24 us (3%)
    pallas_call x1, Pallas kernels, per_device(): pl.pallas_call(functools.partial(kernel, n, cap), out_shape=jax.ShapeDtyp...  181 us
    unnamed x3, local copies, waits for them, and re-layouts  5.24 us

profile of v1, /device:TPU:0, one launch (start us, length us, event | category | flops | bytes accessed | tf_op | source)
XLA Modules:
  0.0 186.1 jit_solution(2565110371851029876)
XLA Ops:
  0.0 1.5 copy.8.ids_ref
  1.5 1.5 copy.9.gw_ref
  2.9 180.9 %shard_map.73 = bf16[256,2048]{1,0:T(8,128)(2,1)} custom-call(bf16[256,2048]{1,0:T(8,128)(2,1)} %tok_ref.1, f32[1,2048]{1,0:T(1,128)} %bitcast.1, s32[256,2]{1,0:T(8,128)} %copy.8.ids_ref, f32[256,2]{1,0:T(8,128)} %copy.9.gw_ref, bf16[1,2048,1024]{2,1,0:T(8,128)(2,1)} %wg_ref.1, bf16[1,2048,1024]{2,1,0:T(8,128)(2,1)} %wu_ref.1, bf16[1,1024,2048]{2,1,0:T(8,128)(2,1)} %wd_ref.1), custom_call_target="tpu_custom_call" | custom-call | tf_op jit(solution)/shard_map/pallas_call | solution.py:376
  183.8 2.3 %copy.11 = bf16[256,2048]{1,0:T(8,128)(2,1)} copy(bf16[256,2048]{1,0:T(8,128)(2,1)} %shard_map.73) | data formatting | bytes 2097152

commit v2 on v1

--- a/solution.py
+++ b/solution.py
@@ -1,4 +1,5 @@
 import functools
+import heapq
 import jax
 import jax.numpy as jnp
 from jax import lax
@@ -9,9 +10,111 @@
 SUB = 4
 KD = 4
 KR = 4
-
-
-def kernel(n, cap, tok_ref, gain_ref, ids_ref, gw_ref, wg_ref, wu_ref, wd_ref, out_ref,
+KINDS = "SZTUDMFX"
+Z_BLOCK, Y_BLOCK, LAG = 23.0, 11.2, 2.0
+COST = {"S": 0.1, "Z": 0.1, "T": 0.9, "U": 3.1, "D": 1.9, "M": 1.2, "F": 1.2}
+RANK = {"S": 0, "Z": 0, "T": 1, "M": 2, "F": 3, "D": 4, "U": 5}
+START, PACK = 6.0, 8.0
+PRIO = {}
+HOLD = {}
+
+
+def tables(zs):
+    need, when, todo = {}, {}, [[] for _ in range(zs)]
+    order = [[] for _ in range(zs)]
+
+    def task(h, name, b, k, deps, at=0.0):
+        need[h, name, b, k], when[h, name, b, k] = deps, at
+        todo[h].append((name, b, k))
+
+    def rule(h, name, b, k):
+        flip = h >= zs / 2
+        if name in "SZ":
+            name = "ZS"["SZ".index(name)] if flip else name
+            return (zs - 1 - h if flip else h), name, k * 4 // KD
+        return (zs - 1 - h, name, zs - 1 - b) if flip else (h, name, b)
+
+    for h in range(zs):
+        for b in range(zs):
+            for k in range(KD):
+                task(h, "T", b, k, int(b != h), PACK if b == h else 0.0)
+            task(h, "U", b, 0, KD)
+            for k in range(KR):
+                task(h, "D", b, k, 1)
+                if b == h:
+                    task(h, "F", b, k, 1 + (h > 0) + (h < zs - 1))
+                else:
+                    task(h, "M", b, k, 1 + (h > 0 if b > h else h < zs - 1))
+        for name, way in (("S", 1), ("Z", 0)):
+            for k in range(KD if (h < zs - 1 if way else h > 0) else 0):
+                task(h, name, h, k, 0, START)
+    events, busy, link = [], [0.0] * zs, {}
+
+    def supply(h, name, b, k, at):
+        need[h, name, b, k] -= 1
+        when[h, name, b, k] = max(when[h, name, b, k], at)
+        heapq.heappush(events, (at, h))
+
+    def wire(key, time, at):
+        link[key] = max(at, link.get(key, 0.0)) + time
+        return link[key] + LAG
+
+    def onward(h, way, b, k, name, time, at):
+        g = h + 2 * way - 1
+        supply(g, "F" if name == "M" and g == b else name, b, k, wire((h, way), time, at))
+
+    for h in range(zs):
+        events += [(START, h), (PACK, h)]
+    heapq.heapify(events)
+    end = 0.0
+    while events:
+        t, h = heapq.heappop(events)
+        if busy[h] > t + 1e-9:
+            continue
+        best, later = None, None
+        for c in todo[h]:
+            if need[(h,) + c] > 0:
+                continue
+            key = rule(h, *c)
+            at = max(when[(h,) + c], HOLD.get(key, 0.0))
+            if at <= t + 1e-9:
+                p = (-1 if c[0] in "SZ" and c[2] == 0 else PRIO.get(key, RANK[c[0]]) + 0.01 * c[2], c)
+                best = min(best, p) if best else p
+            else:
+                later = at if later is None else min(later, at)
+        if best is None:
+            if later is not None:
+                heapq.heappush(events, (later, h))
+            continue
+        name, b, k = best[1]
+        todo[h].remove(best[1])
+        order[h].append(best[1])
+        done = t + 0.1 + COST[name] / {"T": KD, "D": KR, "M": KR, "F": KR}.get(name, 1)
+        if name in "SZ":
+            onward(h, int(name == "S"), b, k, "T", Z_BLOCK / KD, t)
+        elif name == "T":
+            way = int(b < h)
+            if b != h and (h < zs - 1 if way else h > 0):
+                onward(h, way, b, k, "T", Z_BLOCK / KD, t + 0.1)
+            supply(h, "U", b, 0, wire(h, Y_BLOCK / KD, done))
+        elif name == "U":
+            for r in range(KR):
+                supply(h, "D", b, r, done)
+        elif name == "D":
+            supply(h, "F" if b == h else "M", b, k, wire(h, Y_BLOCK / KR, done))
+        elif name == "M":
+            onward(h, int(b > h), b, k, "M", Z_BLOCK / KR, done)
+        end = max(end, done)
+        busy[h] = done
+        heapq.heappush(events, (done, h))
+    assert not any(todo)
+    codes = [[KINDS.index(n) * 1024 + b * 32 + k for n, b, k in o if n not in "SZ" or k > 0]
+             for o in order]
+    size = max(map(len, codes))
+    return [c + [KINDS.index("X") * 1024] * (size - len(c)) for c in codes]
+
+
+def kernel(n, cap, table, tok_ref, gain_ref, ids_ref, gw_ref, wg_ref, wu_ref, wd_ref, out_ref,
            wg, wu, wd, lines, places, outgoing, arrived, results, returned, hidden, chain,
            pick, high, low,
            wsem, lsend, lrecv, psend, precv, dsend, drecv, bsend, brecv, csend, crecv):
@@ -22,7 +125,6 @@
     ff = wg.shape[1]
     rows = SUB * cap
     dcols, rcols = width // KD, width // KR
-    own = 2
 
     def peer(plane, part):
         return {"ep": plane * SUB + part}
@@ -105,6 +207,13 @@
         part = chain.at[way * zs + j, :, rcol(k)]
         return remote(part, part, csend.at[way * zs + j], crecv.at[(way * zs + j) * KR + k],
                       peer(onward(way), lo))
+
+    steps = []
+    for codes in zip(*table):
+        code = jnp.int32(codes[0])
+        for plane in range(1, zs):
+            code = jnp.where(hi == plane, codes[plane], code)
+        steps.append(code)
 
     step = 32
 
@@ -152,8 +261,6 @@
 
     def send_own(way):
         place_copy(hi, way).start()
-        for k in range(1, KD):
-            line_copy(hi, k, way).start()
 
     for way in (1, 0):
         forward(way, send_own)
@@ -178,35 +285,25 @@
 
     ftile = min(ff, 256)
 
-    def experts(j):
-        at = block_rows(j)
-
-        def landed(k, carry):
-            out_arrival(j, k).wait_recv()
-            return carry
-
-        lax.fori_loop(0, KD, landed, 0)
-
-        def up(f, carry):
-            cols = pl.ds(pl.multiple_of(f * ftile, ftile), ftile)
-            x = arrived[at, :]
-            g = jnp.dot(x, wg[:, cols], preferred_element_type=jnp.float32)
-            u = jnp.dot(x, wu[:, cols], preferred_element_type=jnp.float32)
-            hidden[:, cols] = (g / (1.0 + jnp.exp(-g)) * u).astype(jnp.bfloat16)
-            return carry
-
-        lax.fori_loop(0, ff // ftile, up, 0)
-
-        def down(k, carry):
-            got = jnp.dot(hidden[...], wd[:, rcol(k)],
-                          preferred_element_type=jnp.float32).astype(jnp.bfloat16)
-            results[far_rows(j), rcol(k)] = got[cap:, :]
-            for dl in range(1, SUB):
-                back_copy(j, dl, k).start()
-            returned[slot_rows(j, 0), rcol(k)] = got[:cap, :]
-            return carry
-
-        lax.fori_loop(0, KR, down, 0)
+    def landed(j, k, carry):
+        out_arrival(j, k).wait_recv()
+        return carry
+
+    def up(j, f, carry):
+        cols = pl.ds(pl.multiple_of(f * ftile, ftile), ftile)
+        x = arrived[block_rows(j), :]
+        g = jnp.dot(x, wg[:, cols], preferred_element_type=jnp.float32)
+        u = jnp.dot(x, wu[:, cols], preferred_element_type=jnp.float32)
+        hidden[j, :, cols] = (g / (1.0 + jnp.exp(-g)) * u).astype(jnp.bfloat16)
+        return carry
+
+    def down(j, k):
+        got = jnp.dot(hidden[j], wd[:, rcol(k)],
+                      preferred_element_type=jnp.float32).astype(jnp.bfloat16)
+        results[far_rows(j), rcol(k)] = got[cap:, :]
+        for dl in range(1, SUB):
+            back_copy(j, dl, k).start()
+        returned[slot_rows(j, 0), rcol(k)] = got[:cap, :]
 
     def weigh(j, at):
         index = row_index()
@@ -222,118 +319,107 @@
         return (jnp.dot(high[at], block, preferred_element_type=jnp.float32)
                 + jnp.dot(low[at], block, preferred_element_type=jnp.float32))
 
-    choose(hi, own)
-
-    def pack_own(k, carry):
-        pack(hi, k, own)
+    def take(j, k):
+        way = jnp.where(j < hi, 1, 0)
+
+        @pl.when((k == 0) & (j != hi))
+        def _():
+            place_copy(j, way).wait_recv()
+            forward(way, lambda w: place_copy(j, w).start())
+
+        @pl.when(k == 0)
+        def _():
+            choose(j, j)
+
+        @pl.when(j != hi)
+        def _():
+            line_copy(j, k, way).wait_recv()
+            forward(way, lambda w: line_copy(j, k, w).start())
+
+        pack(j, k, j)
+
+    def up_all(j):
+        lax.fori_loop(0, KD, lambda k, c: landed(j, k, c), 0)
+
+        @pl.when(j == hi)
+        def _():
+            for c in w_copies:
+                c.wait()
+
+        lax.fori_loop(0, ff // ftile, lambda f, c: up(j, f, c), 0)
+
+    def add(j, k):
+        way = jnp.where(j > hi, 1, 0)
+
+        @pl.when(k == 0)
+        def _():
+            weigh(j, j)
+
+        back_arrival(j, k).wait_recv()
+        value = mix(j, k, j)
+        at = way * zs + j
+        beyond = way * hi + (1 - way) * (zs - 1 - hi)
+
+        @pl.when(beyond > 0)
+        def _():
+            chain_copy(way, j, k).wait_recv()
+            chain[at, :, rcol(k)] = (
+                value + chain[at, :, rcol(k)].astype(jnp.float32)).astype(jnp.bfloat16)
+
+        @pl.when(beyond == 0)
+        def _():
+            chain[at, :, rcol(k)] = value.astype(jnp.bfloat16)
+
+        chain_copy(way, j, k).start()
+
+    def final(k):
+        @pl.when(k == 0)
+        def _():
+            weigh(hi, hi)
+
+        back_arrival(hi, k).wait_recv()
+        value = mix(hi, k, hi)
+
+        def arrived_from(way):
+            chain_copy(way, hi, k).wait_recv()
+            return chain[way * zs + hi, :, rcol(k)].astype(jnp.float32)
+
+        def put(total):
+            out_ref[:, rcol(k)] = total.astype(out_ref.dtype)
+
+        @pl.when(hi == 0)
+        def _():
+            put(value + arrived_from(0))
+
+        @pl.when(hi == zs - 1)
+        def _():
+            put(value + arrived_from(1))
+
+        @pl.when((hi > 0) & (hi < zs - 1))
+        def _():
+            put(value + arrived_from(0) + arrived_from(1))
+
+    def run(i, carry):
+        code = steps[0]
+        for at in range(1, len(steps)):
+            code = jnp.where(i == at, steps[at], code)
+        kind, j, k = code // 1024, code // 32 % 32, code % 32
+
+        def on(name, act):
+            @pl.when(kind == KINDS.index(name))
+            def _():
+                act()
+
+        on("S", lambda: forward(1, lambda w: line_copy(hi, k, w).start()))
+        on("Z", lambda: forward(0, lambda w: line_copy(hi, k, w).start()))
+        on("T", lambda: take(j, k))
+        on("U", lambda: up_all(j))
+        on("D", lambda: down(j, k))
+        on("M", lambda: add(j, k))
+        on("F", lambda: final(k))
         return carry
 
-    lax.fori_loop(0, KD, pack_own, 0)
-    for c in w_copies:
-        c.wait()
-
-    experts(hi)
-    weigh(hi, own)
-
-    first = hi // ((zs + 1) // 2)
-    ways = (first, 1 - first)
-
-    def arriving(s, act):
-        for way in ways:
-            block = hi + (1 - 2 * way) * s
-
-            @pl.when((block >= 0) & (block < zs))
-            def _():
-                act((block + zs) % zs, way)
-
-    def stage(s):
-        def begin(block, way):
-            place_copy(block, way).wait_recv()
-            forward(way, lambda w: place_copy(block, w).start())
-            choose(block, way)
-
-        arriving(s, begin)
-
-        def chunk(k, carry):
-            def take(block, way):
-                line_copy(block, k, way).wait_recv()
-                forward(way, lambda w: line_copy(block, k, w).start())
-                pack(block, k, way)
-
-            arriving(s, take)
-            return carry
-
-        lax.fori_loop(0, KD, chunk, 0)
-        arriving(s, lambda block, way: experts(block))
-
-    def leaving(t, act):
-        for way in (1, 0):
-            j = way * t + (1 - way) * (zs - 1 - t)
-
-            @pl.when(j > hi if way else j < hi)
-            def _():
-                act(j, way)
-
-    def give(t):
-        leaving(t, lambda j, way: weigh(j, way))
-
-        def chunk(k, carry):
-            def add(j, way):
-                back_arrival(j, k).wait_recv()
-                value = mix(j, k, way)
-                at = way * zs + j
-
-                @pl.when(hi > 0 if way else hi < zs - 1)
-                def _():
-                    chain_copy(way, j, k).wait_recv()
-                    chain[at, :, rcol(k)] = (
-                        value + chain[at, :, rcol(k)].astype(jnp.float32)).astype(jnp.bfloat16)
-
-                @pl.when(hi == 0 if way else hi == zs - 1)
-                def _():
-                    chain[at, :, rcol(k)] = value.astype(jnp.bfloat16)
-
-                chain_copy(way, j, k).start()
-
-            leaving(t, add)
-            return carry
-
-        lax.fori_loop(0, KR, chunk, 0)
-
-    def turn(s, carry):
-        stage(s)
-        give(s)
-        return carry
-
-    lax.fori_loop(1, zs, turn, 0)
-
-    def final(k, carry):
-        back_arrival(hi, k).wait_recv()
-        value = mix(hi, k, own)
-
-        @pl.when(hi == 0)
-        def _():
-            chain_copy(0, hi, k).wait_recv()
-            out_ref[:, rcol(k)] = (
-                value + chain[hi, :, rcol(k)].astype(jnp.float32)).astype(out_ref.dtype)
-
-        @pl.when(hi == zs - 1)
-        def _():
-            chain_copy(1, hi, k).wait_recv()
-            out_ref[:, rcol(k)] = (
-                value + chain[zs + hi, :, rcol(k)].astype(jnp.float32)).astype(out_ref.dtype)
-
-        @pl.when((hi > 0) & (hi < zs - 1))
-        def _():
-            chain_copy(0, hi, k).wait_recv()
-            chain_copy(1, hi, k).wait_recv()
-            out_ref[:, rcol(k)] = (
-                value + chain[hi, :, rcol(k)].astype(jnp.float32)
-                + chain[zs + hi, :, rcol(k)].astype(jnp.float32)).astype(out_ref.dtype)
-
-        return carry
-
-    lax.fori_loop(0, KR, final, 0)
+    lax.fori_loop(0, len(table[0]), run, 0)
 
     def finish(j, carry):
         at = far_rows(j)
@@ -369,12 +455,13 @@
     total = n * cap
     zs = n // SUB
     rows = SUB * cap
+    table = tables(zs)
     bf16 = jnp.bfloat16
     dma = pltpu.SemaphoreType.DMA
     vmem = pl.BlockSpec(memory_space=pltpu.VMEM)
     hbm = pl.BlockSpec(memory_space=pl.ANY)
     return pl.pallas_call(
-        functools.partial(kernel, n, cap),
+        functools.partial(kernel, n, cap, table),
         out_shape=jax.ShapeDtypeStruct((tok, width), bf16),
         in_specs=[vmem] * 4 + [hbm] * 3,
         out_specs=vmem,
@@ -388,11 +475,11 @@
             pltpu.VMEM((total, width), bf16),
             pltpu.VMEM((total, width), bf16),
             pltpu.VMEM((total, width), bf16),
-            pltpu.VMEM((rows, ff), bf16),
+            pltpu.VMEM((zs, rows, ff), bf16),
             pltpu.VMEM((2 * zs, tok, width), bf16),
-            pltpu.VMEM((3, rows, tok), bf16),
-            pltpu.VMEM((3, tok, rows), bf16),
-            pltpu.VMEM((3, tok, rows), bf16),
+            pltpu.VMEM((zs, rows, tok), bf16),
+            pltpu.VMEM((zs, tok, rows), bf16),
+            pltpu.VMEM((zs, tok, rows), bf16),
             dma((3,)),
             dma((2 * zs,)),
             dma((zs * KD,)),

time: 186 us -> 143 us (0.77)
  Pallas kernels: 181 us -> 137 us
    pallas_call x1, Pallas kernels: 181 us -> 137 us  [per_device(): pl.pallas_call(functools.partial(kernel, n, cap, table), out_shape=jax.Sh...]
where the time goes in v2:
time: 143 us; the launch traced here: 142 us
  Pallas kernels  137 us (96%)
  local copies, waits for them, and re-layouts  5.24 us (4%)
    pallas_call x1, Pallas kernels, per_device(): pl.pallas_call(functools.partial(kernel, n, cap, table), out_shape=jax.Sh...  137 us
    unnamed x3, local copies, waits for them, and re-layouts  5.24 us

profile of v2, /device:TPU:0, one launch (start us, length us, event | category | flops | bytes accessed | tf_op | source)
XLA Modules:
  0.0 142.3 jit_solution(6868759689940138824)
XLA Ops:
  0.0 1.5 %copy.8.ids_ref = s32[256,2]{1,0:T(8,128)} copy(s32[256,2]{0,1:T(2,128)} %param.9) | data formatting | bytes 4096 | tf_op args[2]
  1.5 1.5 %copy.9.gw_ref = f32[256,2]{1,0:T(8,128)} copy(f32[256,2]{0,1:T(2,128)} %param.10) | data formatting | bytes 4096 | tf_op args[3]
  2.9 137.1 %shard_map.73 = bf16[256,2048]{1,0:T(8,128)(2,1)} custom-call(bf16[256,2048]{1,0:T(8,128)(2,1)} %tok_ref.1, f32[1,2048]{1,0:T(1,128)} %bitcast.1, s32[256,2]{1,0:T(8,128)} %copy.8.ids_ref, f32[256,2]{1,0:T(8,128)} %copy.9.gw_ref, bf16[1,2048,1024]{2,1,0:T(8,128)(2,1)} %wg_ref.1, bf16[1,2048,1024]{2,1,0:T(8,128)(2,1)} %wu_ref.1, bf16[1,1024,2048]{2,1,0:T(8,128)(2,1)} %wd_ref.1), custom_call_target="tpu_custom_call" | custom-call | tf_op jit(solution)/shard_map/pallas_call | solution.py:463
  140.0 2.3 %copy.11 = bf16[256,2048]{1,0:T(8,128)(2,1)} copy(bf16[256,2048]{1,0:T(8,128)(2,1)} %shard_map.73) | data formatting | bytes 2097152

commit v3 on v2

--- a/solution.py
+++ b/solution.py
@@ -8,33 +8,35 @@
 from jax.sharding import PartitionSpec as P
 
 SUB = 4
-KD = 4
-KR = 4
-KINDS = "SZTUDMFX"
-Z_BLOCK, Y_BLOCK, LAG = 23.0, 11.2, 2.0
-COST = {"S": 0.1, "Z": 0.1, "T": 0.9, "U": 3.1, "D": 1.9, "M": 1.2, "F": 1.2}
+KD = 8
+KR = 8
+PIECES = 4
+KINDS = "SZTUDMFWX"
+COST = {"S": 0.0, "Z": 0.0, "T": 0.9, "U": 3.1, "D": 1.8, "M": 1.25, "F": 1.4}
 RANK = {"S": 0, "Z": 0, "T": 1, "M": 2, "F": 3, "D": 4, "U": 5}
-START, PACK = 6.0, 8.0
-PRIO = {}
-HOLD = {}
+Z_BLOCK, Y_BLOCK, LAG, START, PACK, STEP = 22.6, 11.2, 2.2, 2.9, 3.6, 0.12
+PRIO = {(0, 'D', 2): 4.8, (1, 'U', 3): 4.7, (0, 'U', 1): 0.6}
+HOLD = {(1, 'Z', 1): 54, (1, 'Z', 2): 68, (1, 'Z', 3): 70, (0, 'D', 0): 88, (1, 'U', 1): 68, (1, 'T', 1): 7, (1, 'D', 0): 62}
 
 
 def tables(zs):
-    need, when, todo = {}, {}, [[] for _ in range(zs)]
-    order = [[] for _ in range(zs)]
+    half = zs // 2
+    need, when, ready = {}, {}, [[] for _ in range(half)]
+    order = [[] for _ in range(half)]
+    pieces = {"T": KD, "D": KR, "M": KR, "F": KR}
+
+    def release(h, name, b, k):
+        key = (h, name, k * 4 // KD) if name in "SZ" else (h, name, b)
+        rank = -1.0 if name in "SZ" and k == 0 else PRIO.get(key, RANK[name])
+        at = max(when[h, name, b, k], HOLD.get(key, 0.0))
+        ready[h].append((rank + 0.01 * k, abs(b - h), name, b, k, at))
 
     def task(h, name, b, k, deps, at=0.0):
         need[h, name, b, k], when[h, name, b, k] = deps, at
-        todo[h].append((name, b, k))
-
-    def rule(h, name, b, k):
-        flip = h >= zs / 2
-        if name in "SZ":
-            name = "ZS"["SZ".index(name)] if flip else name
-            return (zs - 1 - h if flip else h), name, k * 4 // KD
-        return (zs - 1 - h, name, zs - 1 - b) if flip else (h, name, b)
-
-    for h in range(zs):
+        if deps == 0:
+            release(h, name, b, k)
+
+    for h in range(half):
         for b in range(zs):
             for k in range(KD):
                 task(h, "T", b, k, int(b != h), PACK if b == h else 0.0)
@@ -45,14 +47,20 @@
                     task(h, "F", b, k, 1 + (h > 0) + (h < zs - 1))
                 else:
                     task(h, "M", b, k, 1 + (h > 0 if b > h else h < zs - 1))
-        for name, way in (("S", 1), ("Z", 0)):
-            for k in range(KD if (h < zs - 1 if way else h > 0) else 0):
-                task(h, name, h, k, 0, START)
-    events, busy, link = [], [0.0] * zs, {}
+        for k in range(KD):
+            task(h, "S", h, k, 0, START)
+            if h > 0:
+                task(h, "Z", h, k, 0, START)
+    busy, link = [0.0] * half, {}
+    events = [(at, h) for at in (START, PACK) for h in range(half)]
 
     def supply(h, name, b, k, at):
+        if h >= half:
+            h, b = zs - 1 - h, zs - 1 - b
         need[h, name, b, k] -= 1
         when[h, name, b, k] = max(when[h, name, b, k], at)
+        if need[h, name, b, k] == 0:
+            release(h, name, b, k)
         heapq.heappush(events, (at, h))
 
     def wire(key, time, at):
@@ -63,35 +71,23 @@
         g = h + 2 * way - 1
         supply(g, "F" if name == "M" and g == b else name, b, k, wire((h, way), time, at))
 
-    for h in range(zs):
-        events += [(START, h), (PACK, h)]
     heapq.heapify(events)
-    end = 0.0
     while events:
         t, h = heapq.heappop(events)
         if busy[h] > t + 1e-9:
             continue
-        best, later = None, None
-        for c in todo[h]:
-            if need[(h,) + c] > 0:
-                continue
-            key = rule(h, *c)
-            at = max(when[(h,) + c], HOLD.get(key, 0.0))
-            if at <= t + 1e-9:
-                p = (-1 if c[0] in "SZ" and c[2] == 0 else PRIO.get(key, RANK[c[0]]) + 0.01 * c[2], c)
-                best = min(best, p) if best else p
-            else:
-                later = at if later is None else min(later, at)
-        if best is None:
-            if later is not None:
-                heapq.heappush(events, (later, h))
+        now = [c for c in ready[h] if c[5] <= t + 1e-9]
+        if not now:
+            if ready[h]:
+                heapq.heappush(events, (min(c[5] for c in ready[h]), h))
             continue
-        name, b, k = best[1]
-        todo[h].remove(best[1])
-        order[h].append(best[1])
-        done = t + 0.1 + COST[name] / {"T": KD, "D": KR, "M": KR, "F": KR}.get(name, 1)
+        best = min(now)
+        ready[h].remove(best)
+        name, b, k = best[2:5]
+        order[h].append((name, b, k))
+        done = t + STEP + COST[name] / pieces.get(name, 1)
         if name in "SZ":
-            onward(h, int(name == "S"), b, k, "T", Z_BLOCK / KD, t)
+            onward(h, int(name == "S"), b, k, "T", Z_BLOCK / KD, t + 0.05)
         elif name == "T":
             way = int(b < h)
             if b != h and (h < zs - 1 if way else h > 0):
@@ -104,20 +100,28 @@
             supply(h, "F" if b == h else "M", b, k, wire(h, Y_BLOCK / KR, done))
         elif name == "M":
             onward(h, int(b > h), b, k, "M", Z_BLOCK / KR, done)
-        end = max(end, done)
         busy[h] = done
         heapq.heappush(events, (done, h))
-    assert not any(todo)
-    codes = [[KINDS.index(n) * 1024 + b * 32 + k for n, b, k in o if n not in "SZ" or k > 0]
-             for o in order]
-    size = max(map(len, codes))
-    return [c + [KINDS.index("X") * 1024] * (size - len(c)) for c in codes]
+    assert sum(map(len, order)) == len(need)
+
+    def code(name, b, k):
+        return KINDS.index(name) * 1024 + b * 32 + k
+
+    def mirror(name, b, k):
+        return {"S": "Z", "Z": "S"}.get(name, name), zs - 1 - b, k
+
+    order = [[c for c in o if c[0] not in "SZ" or c[2] > 0] for o in order]
+    for o in order:
+        o.insert([c[0] for c in o].index("U"), ("W", 0, 0))
+    order += [[mirror(*c) for c in o] for o in reversed(order)]
+    size = max(map(len, order))
+    return [[code(*c) for c in o] + [code("X", 0, 0)] * (size - len(o)) for o in order]
 
 
 def kernel(n, cap, table, tok_ref, gain_ref, ids_ref, gw_ref, wg_ref, wu_ref, wd_ref, out_ref,
            wg, wu, wd, lines, places, outgoing, arrived, results, returned, hidden, chain,
-           pick, high, low,
-           wsem, lsend, lrecv, psend, precv, dsend, drecv, bsend, brecv, csend, crecv):
+           pick, high, low, raw,
+           tsem, wsem, lsend, lrecv, psend, precv, dsend, drecv, bsend, brecv, csend, crecv):
     zs = n // SUB
     me = lax.axis_index("ep")
     hi, lo = me // SUB, me % SUB
@@ -129,6 +133,12 @@
     def peer(plane, part):
         return {"ep": plane * SUB + part}
 
+    pieces = [pl.ds(i * (tok // PIECES), tok // PIECES) for i in range(PIECES)]
+    t_copies = [pltpu.make_async_copy(tok_ref.at[at, :], raw.at[at, :], tsem.at[i])
+                for i, at in enumerate(pieces)]
+    for c in t_copies:
+        c.start()
+
     barrier = pltpu.get_barrier_semaphore()
 
     def greet(to):
@@ -219,12 +229,15 @@
 
     def norm(i, carry):
         at = pl.ds(pl.multiple_of(i * step, step), step)
-        v = tok_ref[at, :].astype(jnp.float32)
+        v = raw[at, :].astype(jnp.float32)
         scale = lax.rsqrt(jnp.mean(v * v, -1, keepdims=True) + 1e-06)
         lines[hi, at, :] = (v * scale * gain_ref[...]).astype(jnp.bfloat16)
         return carry
 
-    lax.fori_loop(0, tok // step, norm, 0)
+    per = tok // PIECES // step
+    for i, c in enumerate(t_copies):
+        c.wait()
+        lax.fori_loop(i * per, (i + 1) * per, norm, 0)
 
     ends = jnp.where(hi == 0, 1, 0) + jnp.where(hi == zs - 1, 1, 0)
     pl.semaphore_wait(barrier, SUB + 1 - ends)
@@ -237,27 +250,22 @@
     for way in (1, 0):
         forward(way, lambda w: line_copy(hi, 0, w).start())
 
-    ids = ids_ref[...]
-    id0, id1 = ids[:, 0:1], ids[:, 1:2]
-    lane = lax.broadcasted_iota(jnp.int32, (tok, 128), 1)
-    chosen = jnp.where((id0 == lane) | (id1 == lane), 1.0, 0.0)
+    expert = lax.broadcasted_iota(jnp.int32, (n, tok), 0)
+    id0, id1 = ids_ref[0:1, :], ids_ref[1:2, :]
+    chosen = jnp.where((id0 == expert) | (id1 == expert), 1.0, 0.0).astype(jnp.bfloat16)
     t_row = lax.broadcasted_iota(jnp.int32, (tok, tok), 0)
     t_col = lax.broadcasted_iota(jnp.int32, (tok, tok), 1)
-    earlier = jnp.where(t_col < t_row, 1.0, 0.0).astype(jnp.bfloat16)
-    before = jnp.dot(earlier, chosen.astype(jnp.bfloat16), preferred_element_type=jnp.float32)
-    slot0 = jnp.sum(jnp.where(id0 == lane, before, 0.0), axis=1, keepdims=True)
-    slot1 = jnp.sum(jnp.where(id1 == lane, before, 0.0), axis=1, keepdims=True)
-    dest0 = id0.astype(jnp.float32) * cap + slot0
-    dest1 = id1.astype(jnp.float32) * cap + slot1
-    gw = gw_ref[...]
-    g0, g1 = gw[:, 0:1], gw[:, 1:2]
-    both = jnp.where(lane == 0, dest0, jnp.where(
-        lane == 1, dest1, jnp.where(lane == 2, g0, jnp.where(lane == 3, g1, 0.0))))
-    turned = jnp.transpose(both)
+    earlier = jnp.where(t_row < t_col, 1.0, 0.0).astype(jnp.bfloat16)
+    before = jnp.dot(chosen, earlier, preferred_element_type=jnp.float32)
+
+    def dest(ids):
+        slot = jnp.sum(jnp.where(ids == expert, before, 0.0), axis=0, keepdims=True)
+        return ids.astype(jnp.float32) * cap + slot
+
     where = lax.broadcasted_iota(jnp.int32, (8, tok), 0)
     places[hi] = jnp.where(
-        where == 0, turned[0:1, :], jnp.where(
-            where == 1, turned[1:2, :], jnp.where(where == 2, turned[2:3, :], turned[3:4, :])))
+        where == 0, dest(id0), jnp.where(
+            where == 1, dest(id1), jnp.where(where == 2, gw_ref[0:1, :], gw_ref[1:2, :])))
 
     def send_own(way):
         place_copy(hi, way).start()
@@ -341,11 +349,6 @@
     def up_all(j):
         lax.fori_loop(0, KD, lambda k, c: landed(j, k, c), 0)
 
-        @pl.when(j == hi)
-        def _():
-            for c in w_copies:
-                c.wait()
-
         lax.fori_loop(0, ff // ftile, lambda f, c: up(j, f, c), 0)
 
     def add(j, k):
@@ -414,6 +417,7 @@
         on("Z", lambda: forward(0, lambda w: line_copy(hi, k, w).start()))
         on("T", lambda: take(j, k))
         on("U", lambda: up_all(j))
+        on("W", lambda: [c.wait() for c in w_copies])
         on("D", lambda: down(j, k))
         on("M", lambda: add(j, k))
         on("F", lambda: final(k))
@@ -462,8 +466,8 @@
     hbm = pl.BlockSpec(memory_space=pl.ANY)
     return pl.pallas_call(
         functools.partial(kernel, n, cap, table),
-        out_shape=jax.ShapeDtypeStruct((tok, width), bf16),
-        in_specs=[vmem] * 4 + [hbm] * 3,
+        out_shape=pltpu.VMEM((tok, width), bf16),
+        in_specs=[hbm] + [vmem] * 3 + [hbm] * 3,
         out_specs=vmem,
         scratch_shapes=[
             pltpu.VMEM((width, ff), bf16),
@@ -480,6 +484,8 @@
             pltpu.VMEM((zs, rows, tok), bf16),
             pltpu.VMEM((zs, tok, rows), bf16),
             pltpu.VMEM((zs, tok, rows), bf16),
+            pltpu.VMEM((tok, width), bf16),
+            dma((PIECES,)),
             dma((3,)),
             dma((2 * zs,)),
             dma((zs * KD,)),
@@ -493,8 +499,8 @@
             dma((2 * zs * KR,)),
         ],
         compiler_params=pltpu.CompilerParams(
-            collective_id=0, has_side_effects=True, vmem_limit_bytes=62 * 1024 * 1024),
-    )(tokens, norm_gain.reshape(1, width), expert_ids, gate_weights, w_gate, w_up, w_down)
+            collective_id=0, has_side_effects=True, vmem_limit_bytes=58 * 1024 * 1024),
+    )(tokens, norm_gain.reshape(1, width), expert_ids.T, gate_weights.T, w_gate, w_up, w_down)
 
 
 def solution(mesh):

time: 143 us -> 128 us (0.90)
  Pallas kernels: 137 us -> 127 us
  local copies, waits for them, and re-layouts: 5.24 us -> 0.97 us
    pallas_call x1, Pallas kernels: 137 us -> 127 us  [per_device(): pl.pallas_call(functools.partial(kernel, n, cap, table), out_shape=pltpu....]
    unnamed x3 -> x1, local copies, waits for them, and re-layouts: 5.24 us -> 0.97 us
where the time goes in v3:
time: 128 us
  Pallas kernels  127 us (99%)
    pallas_call x1, Pallas kernels, per_device(): pl.pallas_call(functools.partial(kernel, n, cap, table), out_shape=pltpu....  127 us

profile of v3, /device:TPU:0, one launch (start us, length us, event | category | flops | bytes accessed | tf_op | source)
XLA Modules:
  0.0 127.6 jit_solution(2002715117842110260)
XLA Ops:
  0.0 126.7 %shard_map.73 = bf16[256,2048]{1,0:T(8,128)(2,1)S(1)} custom-call(bf16[256,2048]{1,0:T(8,128)(2,1)} %tok_ref.1, f32[1,2048]{1,0:T(1,128)} %bitcast.3, s32[2,256]{1,0:T(2,128)} %bitcast.4, f32[2,256]{1,0:T(2,128)} %bitcast.5, bf16[1,2048,1024]{2,1,0:T(8,128)(2,1)} %wg_ref.1, bf16[1,2048,1024]{2,1,0:T(8,128)(2,1)} %wu_ref.1, bf16[1,1024,2048]{2,1,0:T(8,128)(2,1)} %wd_ref.1), custom_call_target="tpu_custom_call" | custom-call | tf_op jit(solution)/shard_map/pallas_call | solution.py:467
  126.7 1.0 copy.9

commit v4 on v3

--- a/solution.py
+++ b/solution.py
@@ -1,3 +1,4 @@
+import bisect
 import functools
 import heapq
 import jax
@@ -11,120 +12,271 @@
 KD = 8
 KR = 8
 PIECES = 4
-KINDS = "SZTUDMFWX"
-COST = {"S": 0.0, "Z": 0.0, "T": 0.9, "U": 3.1, "D": 1.8, "M": 1.25, "F": 1.4}
-RANK = {"S": 0, "Z": 0, "T": 1, "M": 2, "F": 3, "D": 4, "U": 5}
-Z_BLOCK, Y_BLOCK, LAG, START, PACK, STEP = 22.6, 11.2, 2.2, 2.9, 3.6, 0.12
-PRIO = {(0, 'D', 2): 4.8, (1, 'U', 3): 4.7, (0, 'U', 1): 0.6}
-HOLD = {(1, 'Z', 1): 54, (1, 'Z', 2): 68, (1, 'Z', 3): 70, (0, 'D', 0): 88, (1, 'U', 1): 68, (1, 'T', 1): 7, (1, 'D', 0): 62}
-
-
-def tables(zs):
+GROUP = 8
+KINDS = "SZGTUVDEMFWNQX"
+COST = {"T": 1.76, "U": 2.5, "V": 2.5, "D": 1.4, "E": 1.4, "M": 1.9, "F": 2.0}
+RANK = {"S": 0, "Z": 0, "G": 0.5, "T": 1, "N": -1, "M": 2, "F": 3, "D": 4, "E": 4, "U": 5, "V": 5}
+Z_BLOCK, Y_BLOCK, LAG, START, PACK, STEP, BACKLOG = 11.3, 5.6, 2.2, 2.9, 4.6, 0.16, 3.0
+HANDOVER = 2
+PRIO = {(0, 0, 'D', 1): 1.4,
+ (0, 0, 'D', 2): 5.6,
+ (0, 0, 'D', 3): 1.2,
+ (0, 0, 'E', 3): 1.2,
+ (0, 0, 'M', 1): 0.5,
+ (0, 0, 'M', 2): 4.1,
+ (0, 0, 'S', 0): 3.2,
+ (0, 0, 'S', 1): 4.0,
+ (0, 0, 'S', 3): 1.7,
+ (0, 0, 'T', 1): 3.2,
+ (0, 0, 'T', 2): 3.5,
+ (0, 0, 'U', 1): 4.7,
+ (0, 0, 'U', 3): 1.4,
+ (0, 1, 'D', 0): 4.3,
+ (0, 1, 'D', 2): 0.4,
+ (0, 1, 'D', 3): 2.8,
+ (0, 1, 'E', 2): 1.0,
+ (0, 1, 'M', 2): 0.0,
+ (0, 1, 'M', 3): 0.3,
+ (0, 1, 'S', 0): 0.5,
+ (0, 1, 'S', 1): 3.9,
+ (0, 1, 'T', 1): 2.3,
+ (0, 1, 'V', 2): 3.3,
+ (1, 0, 'E', 2): 4.8,
+ (1, 0, 'E', 3): 2.5,
+ (1, 0, 'S', 1): 3.4,
+ (1, 0, 'S', 2): 2.0,
+ (1, 0, 'T', 1): 4.7,
+ (1, 0, 'U', 1): 2.3,
+ (1, 0, 'V', 1): 0.1,
+ (1, 0, 'Z', 1): 0.3,
+ (1, 0, 'Z', 2): 1.8,
+ (1, 1, 'E', 0): 5.5,
+ (1, 1, 'E', 1): 3.0,
+ (1, 1, 'E', 3): 0.2,
+ (1, 1, 'G', 3): 3.5,
+ (1, 1, 'S', 0): 4.1,
+ (1, 1, 'S', 1): 4.5,
+ (1, 1, 'S', 2): 3.7,
+ (1, 1, 'T', 1): 4.7,
+ (1, 1, 'T', 2): 5.0,
+ (1, 1, 'U', 3): 5.5,
+ (1, 1, 'V', 2): 5.4,
+ (1, 1, 'Z', 0): 5.3}
+HOLD = {(0, 0, 'E', 2): 81,
+ (0, 1, 'D', 0): 64,
+ (0, 1, 'S', 3): 23,
+ (0, 1, 'U', 2): 79,
+ (0, 1, 'V', 0): 60,
+ (1, 0, 'D', 3): 52,
+ (1, 0, 'E', 0): 66,
+ (1, 0, 'G', 2): 38,
+ (1, 0, 'S', 0): 26,
+ (1, 0, 'U', 0): 64,
+ (1, 0, 'U', 1): 67,
+ (1, 0, 'U', 3): 34,
+ (1, 0, 'V', 1): 57,
+ (1, 1, 'D', 1): 83,
+ (1, 1, 'S', 3): 29,
+ (1, 1, 'T', 1): 33,
+ (1, 1, 'U', 2): 87,
+ (1, 1, 'Z', 2): 64}
+
+
+def plan(zs):
     half = zs // 2
-    need, when, ready = {}, {}, [[] for _ in range(half)]
-    order = [[] for _ in range(half)]
-    pieces = {"T": KD, "D": KR, "M": KR, "F": KR}
-
-    def release(h, name, b, k):
-        key = (h, name, k * 4 // KD) if name in "SZ" else (h, name, b)
-        rank = -1.0 if name in "SZ" and k == 0 else PRIO.get(key, RANK[name])
-        at = max(when[h, name, b, k], HOLD.get(key, 0.0))
-        ready[h].append((rank + 0.01 * k, abs(b - h), name, b, k, at))
-
-    def task(h, name, b, k, deps, at=0.0):
-        need[h, name, b, k], when[h, name, b, k] = deps, at
+    cores = [(h, c) for h in range(half) for c in (0, 1)]
+    need, when, ready = {}, {}, {d: [] for d in cores}
+    order = {d: [] for d in cores}
+    pieces = {"T": KD, "D": KR, "E": KR, "M": KR, "F": KR}
+    events, busy, links, turn = [], dict.fromkeys(cores, 0.0), {}, [0]
+
+    def post(at, what, key):
+        turn[0] += 1
+        heapq.heappush(events, (at, turn[0], what, key))
+
+    def way_of(h, name, b):
+        if name == "S" or (name == "G" and b < h) or (name == "M" and b > h):
+            return h, 1
+        if name in "ZGM":
+            return h, 0
+        return (h, 2) if name in "DE" else None
+
+    def release(d, name, b, k):
+        key = d + ((name, k * 4 // KD) if name in "SZ" else (name, b))
+        at = max(when[d, name, b, k], HOLD.get(key, 0.0))
+        if name in "SZ" and k + d[1] == 0:
+            key, at = (), START
+        bisect.insort(ready[d], (PRIO.get(key, RANK[name]) + 0.01 * k, abs(b - d[0]), name, b, k,
+                                 at, way_of(d[0], name, b)))
+
+    def task(d, name, b, k, deps, at=0.0):
+        need[d, name, b, k], when[d, name, b, k] = deps, at
         if deps == 0:
-            release(h, name, b, k)
-
-    for h in range(half):
+            release(d, name, b, k)
+
+    for d in cores:
+        h, c = d
         for b in range(zs):
             for k in range(KD):
-                task(h, "T", b, k, int(b != h), PACK if b == h else 0.0)
-            task(h, "U", b, 0, KD)
+                task(d, "T", b, k, int(b != h), PACK if b == h else 0.0)
+                if b != h and (h < zs - 1 if b < h else h > 0):
+                    task(d, "G", b, k, 1)
+            for name, other in (("U", "D"), ("V", "E")):
+                task(d, name, b, 0, KD)
+                for k in range(KR):
+                    task(d, other, b, k, 1)
             for k in range(KR):
-                task(h, "D", b, k, 1)
                 if b == h:
-                    task(h, "F", b, k, 1 + (h > 0) + (h < zs - 1))
+                    task(d, "F", b, k, 2 + (h > 0) + (h < zs - 1))
                 else:
-                    task(h, "M", b, k, 1 + (h > 0 if b > h else h < zs - 1))
+                    task(d, "M", b, k, 2 + (h > 0 if b > h else h < zs - 1))
+        if c == 0:
+            task(d, "N", h + 1, 0, 1)
         for k in range(KD):
-            task(h, "S", h, k, 0, START)
-            if h > 0:
-                task(h, "Z", h, k, 0, START)
-    busy, link = [0.0] * half, {}
-    events = [(at, h) for at in (START, PACK) for h in range(half)]
-
-    def supply(h, name, b, k, at):
-        if h >= half:
-            h, b = zs - 1 - h, zs - 1 - b
-        need[h, name, b, k] -= 1
-        when[h, name, b, k] = max(when[h, name, b, k], at)
-        if need[h, name, b, k] == 0:
-            release(h, name, b, k)
-        heapq.heappush(events, (at, h))
-
-    def wire(key, time, at):
-        link[key] = max(at, link.get(key, 0.0)) + time
-        return link[key] + LAG
-
-    def onward(h, way, b, k, name, time, at):
+            for name in "SZ" if h > 0 else "S":
+                task(d, name, h, k, c + (k > 0), START)
+        post(START, "core", d)
+        post(PACK, "core", d)
+
+    def supply(d, name, b, k, at):
+        if d[0] >= half:
+            d, b = (zs - 1 - d[0], d[1]), zs - 1 - b
+        key = (d, name, b, k)
+        need[key] -= 1
+        when[key] = max(when[key], at)
+        if need[key] == 0:
+            release(*key)
+        post(at, "core", d)
+
+    def settle(key, t):
+        lk = links[key]
+        live = [q for q in lk["queues"] if q]
+        for q in live:
+            q[0][0] -= (t - lk["at"]) / len(live)
+        lk["at"] = t
+        for q in live:
+            while q and q[0][0] <= 1e-6:
+                for e in q.pop(0)[1]:
+                    supply(*e, t + LAG)
+        lk["stamp"] += 1
+        live = [q for q in lk["queues"] if q]
+        if live:
+            post(t + min(q[0][0] for q in live) * len(live), "link", (key, lk["stamp"]))
+
+    def wire(key, c, time, t, targets):
+        lk = links.setdefault(key, {"at": 0.0, "queues": ([], []), "stamp": 0})
+        if any(lk["queues"]):
+            settle(key, t)
+        lk["at"] = t
+        lk["queues"][c].append([time, targets])
+        settle(key, t)
+
+    def backlog(key, c, t):
+        lk = links.get(key)
+        if lk is None:
+            return 0.0
+        return sum(x[0] for x in lk["queues"][c]) * sum(map(bool, lk["queues"]))
+
+    def onward(h, c, way, b, k, name, time, t):
         g = h + 2 * way - 1
-        supply(g, "F" if name == "M" and g == b else name, b, k, wire((h, way), time, at))
-
-    heapq.heapify(events)
+        wire((h, way), c, time, t, [((g, c), "F" if name == "M" and g == b else name, b, k)])
+
+    def pick(d, t):
+        later, full = None, {}
+        for i, x in enumerate(ready[d]):
+            at, gate = x[5:]
+            if at <= t + 1e-9 and gate is not None:
+                if gate not in full:
+                    full[gate] = backlog(gate, d[1], t) - BACKLOG
+                at = t + full[gate] if full[gate] > 1e-6 else at
+            if at <= t + 1e-9:
+                return ready[d].pop(i)[2:5]
+            later = at if later is None else min(later, at)
+        if later is not None:
+            post(max(later, t + 0.1), "core", d)
+        return None
+
     while events:
-        t, h = heapq.heappop(events)
-        if busy[h] > t + 1e-9:
+        t, _, what, key = heapq.heappop(events)
+        if what == "link":
+            if links[key[0]]["stamp"] == key[1]:
+                settle(key[0], t)
             continue
-        now = [c for c in ready[h] if c[5] <= t + 1e-9]
-        if not now:
-            if ready[h]:
-                heapq.heappush(events, (min(c[5] for c in ready[h]), h))
+        d = key
+        if busy[d] > t + 1e-9:
             continue
-        best = min(now)
-        ready[h].remove(best)
-        name, b, k = best[2:5]
-        order[h].append((name, b, k))
-        done = t + STEP + COST[name] / pieces.get(name, 1)
+        choice = pick(d, t)
+        if choice is None:
+            continue
+        h, c = d
+        name, b, k = choice
+        order[d].append(choice)
+        done = t + STEP + COST.get(name, 0.0) / pieces.get(name, 1)
+        done += 0.25 if k == 0 and name in "TM" else 0.0
         if name in "SZ":
-            onward(h, int(name == "S"), b, k, "T", Z_BLOCK / KD, t + 0.05)
+            onward(h, c, int(name == "S"), b, k, "T", Z_BLOCK / KD, t)
+            if k + 1 < KD:
+                supply(d, name, b, k + 1, done)
+        elif name == "G":
+            onward(h, c, int(b < h), b, k, "T", Z_BLOCK / KD, t)
         elif name == "T":
-            way = int(b < h)
-            if b != h and (h < zs - 1 if way else h > 0):
-                onward(h, way, b, k, "T", Z_BLOCK / KD, t + 0.1)
-            supply(h, "U", b, 0, wire(h, Y_BLOCK / KD, done))
-        elif name == "U":
+            if (d, "G", b, k) in need:
+                supply(d, "G", b, k, done)
+            if c == 0 and b == h + 1 and k == KD * HANDOVER // 8:
+                supply(d, "N", b, 0, done)
+            wire((h, 2), c, Y_BLOCK / KD, t, [(d, "U", b, 0), ((h, 1 - c), "V", b, 0)])
+        elif name == "N":
+            for r in range(KD):
+                for s in "SZ" if h > 0 else "S":
+                    supply((h, 1), s, h, r, done + 0.3)
+        elif name in "UV":
             for r in range(KR):
-                supply(h, "D", b, r, done)
-        elif name == "D":
-            supply(h, "F" if b == h else "M", b, k, wire(h, Y_BLOCK / KR, done))
+                supply(d, "D" if name == "U" else "E", b, r, done)
+        elif name in "DE":
+            wire((h, 2), c, Y_BLOCK / KR / 2, t + STEP,
+                 [((h, c if name == "D" else 1 - c), "F" if b == h else "M", b, k)])
         elif name == "M":
-            onward(h, int(b > h), b, k, "M", Z_BLOCK / KR, done)
-        busy[h] = done
-        heapq.heappush(events, (done, h))
-    assert sum(map(len, order)) == len(need)
+            onward(h, c, int(b > h), b, k, "M", Z_BLOCK / KR, t + STEP)
+        busy[d] = done
+        post(done, "core", d)
+    assert sum(map(len, order.values())) == len(need)
+    return order
+
+
+def tables(zs):
+    order = plan(zs)
 
     def code(name, b, k):
-        return KINDS.index(name) * 1024 + b * 32 + k
-
-    def mirror(name, b, k):
-        return {"S": "Z", "Z": "S"}.get(name, name), zs - 1 - b, k
-
-    order = [[c for c in o if c[0] not in "SZ" or c[2] > 0] for o in order]
-    for o in order:
-        o.insert([c[0] for c in o].index("U"), ("W", 0, 0))
-    order += [[mirror(*c) for c in o] for o in reversed(order)]
-    size = max(map(len, order))
-    return [[code(*c) for c in o] + [code("X", 0, 0)] * (size - len(o)) for o in order]
+        return (KINDS.index(name) * zs + b) * max(KD, KR) + k
+
+    def listed(h, c):
+        todo = list(order[min(h, zs - 1 - h), c])
+        if h >= zs // 2:
+            todo = [({"S": "Z", "Z": "S"}.get(name, name), zs - 1 - b, k) for name, b, k in todo]
+        if c == 0:
+            todo = [x for x in todo if x[0] not in "SZ" or x[2] > 0]
+        names = [x[0] for x in todo]
+        first = min(names.index("U"), names.index("V"))
+        todo.insert(first, ("W", 0, 0))
+        if c == 1:
+            turn = min(i for i, x in enumerate(todo) if x[0] in "SZ")
+            todo.insert(turn, ("Q", 0, 0))
+        return todo
+
+    lists = [listed(h, c) for h in range(zs) for c in (0, 1)]
+    size = max(map(len, lists))
+    size += -size % 3
+    return [[code(*x) for x in o] + [code("X", 0, 0)] * (size - len(o)) for o in lists]
 
 
 def kernel(n, cap, table, tok_ref, gain_ref, ids_ref, gw_ref, wg_ref, wu_ref, wd_ref, out_ref,
            wg, wu, wd, lines, places, outgoing, arrived, results, returned, hidden, chain,
            pick, high, low, raw,
-           tsem, wsem, lsend, lrecv, psend, precv, dsend, drecv, bsend, brecv, csend, crecv):
+           tsem, wsem, lsend, lrecv, psend, precv, dsend, drecv, bsend, brecv, csend, crecv, turn):
     zs = n // SUB
     me = lax.axis_index("ep")
     hi, lo = me // SUB, me % SUB
+    core = lo % 2
     tok, width = tok_ref.shape
     ff = wg.shape[1]
     rows = SUB * cap
@@ -175,7 +327,10 @@
         return pl.ds(pl.multiple_of(k * rcols, rcols), rcols)
 
     def slot_rows(j, dl):
-        return pl.ds(pl.multiple_of(j * rows + dl * cap, cap), cap)
+        return pl.ds(pl.multiple_of(j * rows + (dl // 2 + dl % 2 * 2) * cap, cap), cap)
+
+    def side_rows(j, side):
+        return pl.ds(pl.multiple_of(j * rows + side * 2 * cap, 2 * cap), 2 * cap)
 
     def block_rows(j):
         return pl.ds(pl.multiple_of(j * rows, rows), rows)
@@ -198,11 +353,12 @@
     def out_copy(j, dl, k):
         at = slot_rows(j, dl)
         return remote(outgoing.at[at, dcol(k)], arrived.at[at, dcol(k)],
-                      dsend.at[j], drecv.at[j * KD + k], peer(hi, (lo + dl) % SUB))
-
-    def out_arrival(j, k):
-        at = arrived.at[far_rows(j), dcol(k)]
-        return remote(at, at, dsend.at[j], drecv.at[j * KD + k], peer(hi, (lo + 1) % SUB))
+                      dsend.at[j], drecv.at[(j * 2 + dl % 2) * KD + k], peer(hi, (lo + dl) % SUB))
+
+    def out_arrival(j, side, k):
+        at = arrived.at[side_rows(j, 1) if side else slot_rows(j, 2), dcol(k)]
+        return remote(at, at, dsend.at[j], drecv.at[(j * 2 + side) * KD + k],
+                      peer(hi, (lo + 1) % SUB))
 
     def back_copy(j, dl, k):
         at = slot_rows(j, dl)
@@ -218,12 +374,18 @@
         return remote(part, part, csend.at[way * zs + j], crecv.at[(way * zs + j) * KR + k],
                       peer(onward(way), lo))
 
-    steps = []
-    for codes in zip(*table):
-        code = jnp.int32(codes[0])
-        for plane in range(1, zs):
-            code = jnp.where(hi == plane, codes[plane], code)
-        steps.append(code)
+    bits = (len(KINDS) * zs * max(KD, KR) - 1).bit_length()
+    many = 30 // bits
+    idle = KINDS.index("X") * zs * max(KD, KR)
+    where_am_i = hi * 2 + core
+    words = []
+    for i in range(0, len(table[0]), many):
+        packed = [sum(x << bits * r for r, x in enumerate(row[i:i + many])) for row in table]
+        word = jnp.int32(packed[0])
+        for at in range(1, 2 * zs):
+            word = jnp.where(where_am_i == at, packed[at], word)
+        words.append(word)
+    words += [jnp.int32(sum(idle << bits * r for r in range(many)))] * (-len(words) % GROUP)
 
     step = 32
 
@@ -247,8 +409,16 @@
         def _():
             act(way)
 
-    for way in (1, 0):
-        forward(way, lambda w: line_copy(hi, 0, w).start())
+    def send_own(way, k):
+        forward(way, lambda w: line_copy(hi, k, w).start())
+
+    def send_places(way):
+        forward(way, lambda w: place_copy(hi, w).start())
+
+    @pl.when(core == 0)
+    def _():
+        for way in (1, 0):
+            send_own(way, 0)
 
     expert = lax.broadcasted_iota(jnp.int32, (n, tok), 0)
     id0, id1 = ids_ref[0:1, :], ids_ref[1:2, :]
@@ -267,15 +437,22 @@
         where == 0, dest(id0), jnp.where(
             where == 1, dest(id1), jnp.where(where == 2, gw_ref[0:1, :], gw_ref[1:2, :])))
 
-    def send_own(way):
-        place_copy(hi, way).start()
-
-    for way in (1, 0):
-        forward(way, send_own)
+    @pl.when(core == 0)
+    def _():
+        for way in (1, 0):
+            send_places(way)
+
+    def send_line(way, k):
+        @pl.when((core == 1) & (k == 0))
+        def _():
+            send_places(way)
+
+        send_own(way, k)
 
     def row_index():
         r = lax.broadcasted_iota(jnp.int32, (rows, tok), 0)
-        return ((hi * SUB + (lo + r // cap) % SUB) * cap + r % cap).astype(jnp.float32)
+        dl = r // cap % 2 * 2 + r // cap // 2
+        return ((hi * SUB + (lo + dl) % SUB) * cap + r % cap).astype(jnp.float32)
 
     def choose(j, at):
         index = row_index()
@@ -293,25 +470,41 @@
 
     ftile = min(ff, 256)
 
-    def landed(j, k, carry):
-        out_arrival(j, k).wait_recv()
-        return carry
-
-    def up(j, f, carry):
-        cols = pl.ds(pl.multiple_of(f * ftile, ftile), ftile)
-        x = arrived[block_rows(j), :]
-        g = jnp.dot(x, wg[:, cols], preferred_element_type=jnp.float32)
-        u = jnp.dot(x, wu[:, cols], preferred_element_type=jnp.float32)
-        hidden[j, :, cols] = (g / (1.0 + jnp.exp(-g)) * u).astype(jnp.bfloat16)
-        return carry
-
-    def down(j, k):
-        got = jnp.dot(hidden[j], wd[:, rcol(k)],
+    def up(j, side):
+        for which in (0, 1):
+            @pl.when(side == which)
+            def _():
+                def landed(k, carry):
+                    out_arrival(j, which, k).wait_recv()
+                    return carry
+
+                lax.fori_loop(0, KD, landed, 0)
+
+        def tile(f, carry):
+            cols = pl.ds(pl.multiple_of(f * ftile, ftile), ftile)
+            x = arrived[side_rows(j, side), :]
+            g = jnp.dot(x, wg[:, cols], preferred_element_type=jnp.float32)
+            u = jnp.dot(x, wu[:, cols], preferred_element_type=jnp.float32)
+            hidden[j * 2 + side, :, cols] = (g / (1.0 + jnp.exp(-g)) * u).astype(jnp.bfloat16)
+            return carry
+
+        lax.fori_loop(0, ff // ftile, tile, 0)
+
+    def down(j, side, k):
+        got = jnp.dot(hidden[j * 2 + side], wd[:, rcol(k)],
                       preferred_element_type=jnp.float32).astype(jnp.bfloat16)
-        results[far_rows(j), rcol(k)] = got[cap:, :]
-        for dl in range(1, SUB):
-            back_copy(j, dl, k).start()
-        returned[slot_rows(j, 0), rcol(k)] = got[:cap, :]
+
+        @pl.when(side == 0)
+        def _():
+            results[slot_rows(j, 2), rcol(k)] = got[cap:, :]
+            back_copy(j, 2, k).start()
+            returned[slot_rows(j, 0), rcol(k)] = got[:cap, :]
+
+        @pl.when(side == 1)
+        def _():
+            results[side_rows(j, 1), rcol(k)] = got
+            for dl in (1, 3):
+                back_copy(j, dl, k).start()
 
     def weigh(j, at):
         index = row_index()
@@ -333,7 +526,6 @@
         @pl.when((k == 0) & (j != hi))
         def _():
             place_copy(j, way).wait_recv()
-            forward(way, lambda w: place_copy(j, w).start())
 
         @pl.when(k == 0)
         def _():
@@ -342,14 +534,17 @@
         @pl.when(j != hi)
         def _():
             line_copy(j, k, way).wait_recv()
-            forward(way, lambda w: line_copy(j, k, w).start())
 
         pack(j, k, j)
 
-    def up_all(j):
-        lax.fori_loop(0, KD, lambda k, c: landed(j, k, c), 0)
-
-        lax.fori_loop(0, ff // ftile, lambda f, c: up(j, f, c), 0)
+    def pass_on(j, k):
+        way = jnp.where(j < hi, 1, 0)
+
+        @pl.when(k == 0)
+        def _():
+            place_copy(j, way).start()
+
+        line_copy(j, k, way).start()
 
     def add(j, k):
         way = jnp.where(j > hi, 1, 0)
@@ -402,28 +597,55 @@
         def _():
             put(value + arrived_from(0) + arrived_from(1))
 
-    def run(i, carry):
-        code = steps[0]
-        for at in range(1, len(steps)):
-            code = jnp.where(i == at, steps[at], code)
-        kind, j, k = code // 1024, code // 32 % 32, code % 32
-
-        def on(name, act):
-            @pl.when(kind == KINDS.index(name))
-            def _():
-                act()
-
-        on("S", lambda: forward(1, lambda w: line_copy(hi, k, w).start()))
-        on("Z", lambda: forward(0, lambda w: line_copy(hi, k, w).start()))
-        on("T", lambda: take(j, k))
-        on("U", lambda: up_all(j))
-        on("W", lambda: [c.wait() for c in w_copies])
-        on("D", lambda: down(j, k))
-        on("M", lambda: add(j, k))
-        on("F", lambda: final(k))
+    def run(near, i, carry):
+        spot, digit = lax.div(i, many), lax.rem(i, many)
+        word = near[0]
+        for at in range(1, len(near)):
+            word = jnp.where(spot == at, near[at], word)
+        for r in range(1, many):
+            word = jnp.where(digit >= r, lax.div(word, 1 << bits), word)
+        code = lax.rem(word, 1 << bits)
+        kind = lax.div(code, zs * max(KD, KR))
+        j = lax.rem(lax.div(code, max(KD, KR)), zs)
+        k = lax.rem(code, max(KD, KR))
+
+        acts = {
+            "S": lambda: send_line(1, k),
+            "Z": lambda: send_line(0, k),
+            "G": lambda: pass_on(j, k),
+            "T": lambda: take(j, k),
+            "U": lambda: up(j, kind - KINDS.index("U")),
+            "D": lambda: down(j, kind - KINDS.index("D"), k),
+            "M": lambda: add(j, k),
+            "F": lambda: final(k),
+            "W": lambda: [c.wait() for c in w_copies],
+            "N": lambda: pl.semaphore_signal(
+                turn, inc=1, device_id=peer(hi, lo + 1), device_id_type=pl.DeviceIdType.MESH),
+            "Q": lambda: pl.semaphore_wait(turn, 1),
+        }
+
+        def among(names):
+            if len(names) == 1:
+                acts[names[0]]()
+                return
+            cut = len(names) // 2
+            low = kind < KINDS.index(names[cut])
+            pl.when(low)(lambda: among(names[:cut]))
+            pl.when(jnp.logical_not(low))(lambda: among(names[cut:]))
+
+        pl.when(kind < KINDS.index("X"))(lambda: among(list(acts)))
         return carry
 
-    lax.fori_loop(0, len(table[0]), run, 0)
+    def turns(a, carry):
+        near = []
+        for r in range(GROUP):
+            word = words[r]
+            for at in range(1, len(words) // GROUP):
+                word = jnp.where(a == at, words[at * GROUP + r], word)
+            near.append(word)
+        return lax.fori_loop(0, GROUP * many, functools.partial(run, near), carry)
+
+    lax.fori_loop(0, len(words) // GROUP, turns, 0)
 
     def finish(j, carry):
         at = far_rows(j)
@@ -479,7 +701,7 @@
             pltpu.VMEM((total, width), bf16),
             pltpu.VMEM((total, width), bf16),
             pltpu.VMEM((total, width), bf16),
-            pltpu.VMEM((zs, rows, ff), bf16),
+            pltpu.VMEM((2 * zs, rows // 2, ff), bf16),
             pltpu.VMEM((2 * zs, tok, width), bf16),
             pltpu.VMEM((zs, rows, tok), bf16),
             pltpu.VMEM((zs, tok, rows), bf16),
@@ -492,11 +714,12 @@
             dma((2 * zs,)),
             dma((zs,)),
             dma((zs,)),
-            dma((zs * KD,)),
+            dma((2 * zs * KD,)),
             dma((zs,)),
             dma((zs * KR,)),
             dma((2 * zs,)),
             dma((2 * zs * KR,)),
+            pltpu.SemaphoreType.REGULAR,
         ],
         compiler_params=pltpu.CompilerParams(
             collective_id=0, has_side_effects=True, vmem_limit_bytes=58 * 1024 * 1024),

time: 128 us -> 133 us (1.039)
  the two profiles are of different devices: /device:TPU:0 before, /device:TPU:1 now
where the time goes in v4:
time: 133 us
  Pallas kernels  132 us (99%)
    pallas_call x1, Pallas kernels, per_device(): pl.pallas_call(functools.partial(kernel, n, cap, table), out_shape=pltpu....  132 us

profile of v4, /device:TPU:1, one launch (start us, length us, event | category | flops | bytes accessed | tf_op | source)
XLA Modules:
  0.0 133.1 jit_solution(11073845373841990543)
XLA Ops:
  0.0 132.1 %shard_map.73 = bf16[256,2048]{1,0:T(8,128)(2,1)S(1)} custom-call(bf16[256,2048]{1,0:T(8,128)(2,1)} %tok_ref.1, f32[1,2048]{1,0:T(1,128)} %bitcast.3, s32[2,256]{1,0:T(2,128)} %bitcast.4, f32[2,256]{1,0:T(2,128)} %bitcast.5, bf16[1,2048,1024]{2,1,0:T(8,128)(2,1)} %wg_ref.1, bf16[1,2048,1024]{2,1,0:T(8,128)(2,1)} %wu_ref.1, bf16[1,1024,2048]{2,1,0:T(8,128)(2,1)} %wd_ref.1), custom_call_target="tpu_custom_call" | custom-call | tf_op jit(solution)/shard_map/pallas_call | solution.py:689
  132.1 1.0 copy.9

commit v5 on v4

--- a/solution.py
+++ b/solution.py
@@ -14,72 +14,46 @@
 PIECES = 4
 GROUP = 8
 KINDS = "SZGTUVDEMFWNQX"
-COST = {"T": 1.76, "U": 2.5, "V": 2.5, "D": 1.4, "E": 1.4, "M": 1.9, "F": 2.0}
+COST = {"T": 1.6, "U": 2.05, "V": 2.05, "D": 1.96, "E": 1.96, "M": 1.84, "F": 1.7, "G": 0.15, "S": 0.1, "Z": 0.1}
 RANK = {"S": 0, "Z": 0, "G": 0.5, "T": 1, "N": -1, "M": 2, "F": 3, "D": 4, "E": 4, "U": 5, "V": 5}
-Z_BLOCK, Y_BLOCK, LAG, START, PACK, STEP, BACKLOG = 11.3, 5.6, 2.2, 2.9, 4.6, 0.16, 3.0
-HANDOVER = 2
-PRIO = {(0, 0, 'D', 1): 1.4,
- (0, 0, 'D', 2): 5.6,
- (0, 0, 'D', 3): 1.2,
- (0, 0, 'E', 3): 1.2,
- (0, 0, 'M', 1): 0.5,
- (0, 0, 'M', 2): 4.1,
- (0, 0, 'S', 0): 3.2,
- (0, 0, 'S', 1): 4.0,
- (0, 0, 'S', 3): 1.7,
- (0, 0, 'T', 1): 3.2,
- (0, 0, 'T', 2): 3.5,
- (0, 0, 'U', 1): 4.7,
- (0, 0, 'U', 3): 1.4,
- (0, 1, 'D', 0): 4.3,
- (0, 1, 'D', 2): 0.4,
- (0, 1, 'D', 3): 2.8,
- (0, 1, 'E', 2): 1.0,
- (0, 1, 'M', 2): 0.0,
- (0, 1, 'M', 3): 0.3,
- (0, 1, 'S', 0): 0.5,
- (0, 1, 'S', 1): 3.9,
- (0, 1, 'T', 1): 2.3,
- (0, 1, 'V', 2): 3.3,
- (1, 0, 'E', 2): 4.8,
- (1, 0, 'E', 3): 2.5,
- (1, 0, 'S', 1): 3.4,
- (1, 0, 'S', 2): 2.0,
- (1, 0, 'T', 1): 4.7,
- (1, 0, 'U', 1): 2.3,
- (1, 0, 'V', 1): 0.1,
- (1, 0, 'Z', 1): 0.3,
- (1, 0, 'Z', 2): 1.8,
- (1, 1, 'E', 0): 5.5,
- (1, 1, 'E', 1): 3.0,
+Z_BLOCK, Y_BLOCK, LAG, START, PACK, STEP, BACKLOG = 11.3, 5.6, 2.2, 2.9, 3.8, 0.09, 3.0
+HANDOVER = 1
+PRIO = {(0, 0, 'T', 2): 2.3,
+ (0, 1, 'D', 0): 4.5,
+ (0, 1, 'M', 2): 1.0,
+ (0, 1, 'T', 2): 4.9,
+ (1, 0, 'D', 0): 1.8,
+ (1, 0, 'E', 1): 1.8,
+ (1, 0, 'E', 2): 6.0,
+ (1, 0, 'T', 2): 6.0,
+ (1, 0, 'Z', 2): 2.6,
+ (1, 1, 'D', 1): 3.4,
+ (1, 1, 'D', 2): 4.7,
+ (1, 1, 'D', 3): 3.5,
  (1, 1, 'E', 3): 0.2,
- (1, 1, 'G', 3): 3.5,
- (1, 1, 'S', 0): 4.1,
- (1, 1, 'S', 1): 4.5,
- (1, 1, 'S', 2): 3.7,
- (1, 1, 'T', 1): 4.7,
- (1, 1, 'T', 2): 5.0,
- (1, 1, 'U', 3): 5.5,
- (1, 1, 'V', 2): 5.4,
- (1, 1, 'Z', 0): 5.3}
-HOLD = {(0, 0, 'E', 2): 81,
- (0, 1, 'D', 0): 64,
- (0, 1, 'S', 3): 23,
- (0, 1, 'U', 2): 79,
- (0, 1, 'V', 0): 60,
- (1, 0, 'D', 3): 52,
- (1, 0, 'E', 0): 66,
- (1, 0, 'G', 2): 38,
+ (1, 1, 'S', 0): 2.3,
+ (1, 1, 'S', 1): 2.0,
+ (1, 1, 'S', 3): 4.5,
+ (1, 1, 'T', 0): 3.6,
+ (1, 1, 'V', 0): 2.0,
+ (1, 1, 'V', 1): 2.2,
+ (1, 1, 'V', 3): 1.8,
+ (1, 1, 'Z', 0): 3.7,
+ (1, 1, 'Z', 1): 4.0}
+HOLD = {(0, 0, 'U', 0): 86,
+ (0, 1, 'E', 0): 86,
+ (0, 1, 'U', 0): 85,
+ (1, 0, 'D', 1): 82,
+ (1, 0, 'E', 0): 70,
+ (1, 0, 'G', 2): 30,
  (1, 0, 'S', 0): 26,
  (1, 0, 'U', 0): 64,
- (1, 0, 'U', 1): 67,
  (1, 0, 'U', 3): 34,
- (1, 0, 'V', 1): 57,
- (1, 1, 'D', 1): 83,
- (1, 1, 'S', 3): 29,
- (1, 1, 'T', 1): 33,
- (1, 1, 'U', 2): 87,
- (1, 1, 'Z', 2): 64}
+ (1, 0, 'V', 1): 66,
+ (1, 1, 'E', 0): 65,
+ (1, 1, 'T', 1): 32,
+ (1, 1, 'V', 1): 82,
+ (1, 1, 'Z', 0): 56}
 
 
 def plan(zs):
@@ -212,7 +186,7 @@
         name, b, k = choice
         order[d].append(choice)
         done = t + STEP + COST.get(name, 0.0) / pieces.get(name, 1)
-        done += 0.25 if k == 0 and name in "TM" else 0.0
+        done += 0.3 if k == 0 and name in "TM" else 0.0
         if name in "SZ":
             onward(h, c, int(name == "S"), b, k, "T", Z_BLOCK / KD, t)
             if k + 1 < KD:

time: 133 us -> 115 us (0.86)
  the two profiles are of different devices: /device:TPU:1 before, /device:TPU:9 now
where the time goes in v5:
time: 115 us; the launch traced here: 114 us
  Pallas kernels  113 us (98%)
    pallas_call x1, Pallas kernels, per_device(): pl.pallas_call(functools.partial(kernel, n, cap, table), out_shape=pltpu....  113 us

profile of v5, /device:TPU:9, one launch (start us, length us, event | category | flops | bytes accessed | tf_op | source)
XLA Modules:
  0.0 114.5 jit_solution(13503928806039130894)
XLA Ops:
  0.0 113.5 %shard_map.73 = bf16[256,2048]{1,0:T(8,128)(2,1)S(1)} custom-call(bf16[256,2048]{1,0:T(8,128)(2,1)} %tok_ref.1, f32[1,2048]{1,0:T(1,128)} %bitcast.3, s32[2,256]{1,0:T(2,128)} %bitcast.4, f32[2,256]{1,0:T(2,128)} %bitcast.5, bf16[1,2048,1024]{2,1,0:T(8,128)(2,1)} %wg_ref.1, bf16[1,2048,1024]{2,1,0:T(8,128)(2,1)} %wu_ref.1, bf16[1,1024,2048]{2,1,0:T(8,128)(2,1)} %wd_ref.1), custom_call_target="tpu_custom_call" | custom-call | tf_op jit(solution)/shard_map/pallas_call | solution.py:663
  113.5 1.0 copy.9

commit v6 on v5

--- a/solution.py
+++ b/solution.py
@@ -13,47 +13,52 @@
 KR = 8
 PIECES = 4
 GROUP = 8
-KINDS = "SZGTUVDEMFWNQX"
+KINDS = "SZGTUVDEMFWNQ"
 COST = {"T": 1.6, "U": 2.05, "V": 2.05, "D": 1.96, "E": 1.96, "M": 1.84, "F": 1.7, "G": 0.15, "S": 0.1, "Z": 0.1}
 RANK = {"S": 0, "Z": 0, "G": 0.5, "T": 1, "N": -1, "M": 2, "F": 3, "D": 4, "E": 4, "U": 5, "V": 5}
-Z_BLOCK, Y_BLOCK, LAG, START, PACK, STEP, BACKLOG = 11.3, 5.6, 2.2, 2.9, 3.8, 0.09, 3.0
-HANDOVER = 1
-PRIO = {(0, 0, 'T', 2): 2.3,
- (0, 1, 'D', 0): 4.5,
- (0, 1, 'M', 2): 1.0,
- (0, 1, 'T', 2): 4.9,
- (1, 0, 'D', 0): 1.8,
- (1, 0, 'E', 1): 1.8,
- (1, 0, 'E', 2): 6.0,
- (1, 0, 'T', 2): 6.0,
- (1, 0, 'Z', 2): 2.6,
- (1, 1, 'D', 1): 3.4,
- (1, 1, 'D', 2): 4.7,
- (1, 1, 'D', 3): 3.5,
- (1, 1, 'E', 3): 0.2,
- (1, 1, 'S', 0): 2.3,
- (1, 1, 'S', 1): 2.0,
- (1, 1, 'S', 3): 4.5,
- (1, 1, 'T', 0): 3.6,
- (1, 1, 'V', 0): 2.0,
- (1, 1, 'V', 1): 2.2,
- (1, 1, 'V', 3): 1.8,
- (1, 1, 'Z', 0): 3.7,
- (1, 1, 'Z', 1): 4.0}
-HOLD = {(0, 0, 'U', 0): 86,
- (0, 1, 'E', 0): 86,
- (0, 1, 'U', 0): 85,
- (1, 0, 'D', 1): 82,
- (1, 0, 'E', 0): 70,
- (1, 0, 'G', 2): 30,
- (1, 0, 'S', 0): 26,
- (1, 0, 'U', 0): 64,
- (1, 0, 'U', 3): 34,
- (1, 0, 'V', 1): 66,
- (1, 1, 'E', 0): 65,
- (1, 1, 'T', 1): 32,
- (1, 1, 'V', 1): 82,
- (1, 1, 'Z', 0): 56}
+Z_BLOCK, Y_BLOCK, START, PACK, STEP, BACKLOG = 11.3, 5.6, 2.9, 3.8, 0.09, 3.0
+LAG = (2.2, 2.2, 2.2)
+HANDOVER = 4
+PRIO = {(0, 0, 'E', 0): 0.8,
+ (0, 0, 'M', 1): 5.6,
+ (0, 1, 'D', 0): 4.8,
+ (0, 1, 'T', 1): 5.1,
+ (0, 1, 'T', 2): 4.6,
+ (0, 1, 'V', 0): 0.3,
+ (0, 1, 'V', 1): 1.0,
+ (1, 0, 'E', 1): 4.9,
+ (1, 0, 'G', 0): 2.1,
+ (1, 0, 'M', 2): 5.8,
+ (1, 0, 'M', 3): 0.2,
+ (1, 0, 'S', 1): 4.2,
+ (1, 0, 'T', 2): 0.7,
+ (1, 0, 'U', 0): 6.0,
+ (1, 0, 'V', 0): 2.9,
+ (1, 1, 'E', 0): 0.5,
+ (1, 1, 'E', 1): 6.0,
+ (1, 1, 'E', 2): 0.4,
+ (1, 1, 'E', 3): 2.6,
+ (1, 1, 'G', 2): 1.1,
+ (1, 1, 'G', 3): 2.6,
+ (1, 1, 'S', 3): 2.3,
+ (1, 1, 'T', 0): 2.6,
+ (1, 1, 'T', 1): 5.9,
+ (1, 1, 'T', 3): 4.9,
+ (1, 1, 'Z', 0): 5.4}
+HOLD = {(0, 0, 'D', 0): 82,
+ (0, 0, 'E', 0): 95,
+ (0, 0, 'T', 2): 42,
+ (0, 0, 'U', 3): 38,
+ (0, 1, 'E', 0): 93,
+ (1, 0, 'D', 1): 91,
+ (1, 0, 'G', 2): 29,
+ (1, 0, 'S', 0): 27,
+ (1, 0, 'T', 1): 36,
+ (1, 0, 'U', 0): 69,
+ (1, 0, 'V', 0): 69,
+ (1, 1, 'E', 0): 64,
+ (1, 1, 'E', 2): 64,
+ (1, 1, 'T', 1): 65}
 
 
 def plan(zs):
@@ -131,7 +136,7 @@
         for q in live:
             while q and q[0][0] <= 1e-6:
                 for e in q.pop(0)[1]:
-                    supply(*e, t + LAG)
+                    supply(*e, t + LAG[key[1]])
         lk["stamp"] += 1
         live = [q for q in lk["queues"] if q]
         if live:
@@ -238,9 +243,7 @@
         return todo
 
     lists = [listed(h, c) for h in range(zs) for c in (0, 1)]
-    size = max(map(len, lists))
-    size += -size % 3
-    return [[code(*x) for x in o] + [code("X", 0, 0)] * (size - len(o)) for o in lists]
+    return [[code(*x) for x in o] for o in lists]
 
 
 def kernel(n, cap, table, tok_ref, gain_ref, ids_ref, gw_ref, wg_ref, wu_ref, wd_ref, out_ref,
@@ -250,7 +253,7 @@
     zs = n // SUB
     me = lax.axis_index("ep")
     hi, lo = me // SUB, me % SUB
-    core = lo % 2
+    core = (lo + 1) % 2
     tok, width = tok_ref.shape
     ff = wg.shape[1]
     rows = SUB * cap
@@ -350,16 +353,18 @@
 
     bits = (len(KINDS) * zs * max(KD, KR) - 1).bit_length()
     many = 30 // bits
-    idle = KINDS.index("X") * zs * max(KD, KR)
     where_am_i = hi * 2 + core
     words = []
-    for i in range(0, len(table[0]), many):
+    for i in range(0, max(map(len, table)), many):
         packed = [sum(x << bits * r for r, x in enumerate(row[i:i + many])) for row in table]
         word = jnp.int32(packed[0])
         for at in range(1, 2 * zs):
             word = jnp.where(where_am_i == at, packed[at], word)
         words.append(word)
-    words += [jnp.int32(sum(idle << bits * r for r in range(many)))] * (-len(words) % GROUP)
+    words += [jnp.int32(0)] * (-len(words) % GROUP)
+    count = jnp.int32(len(table[0]))
+    for at in range(1, 2 * zs):
+        count = jnp.where(where_am_i == at, len(table[at]), count)
 
     step = 32
 
@@ -594,7 +599,7 @@
             "F": lambda: final(k),
             "W": lambda: [c.wait() for c in w_copies],
             "N": lambda: pl.semaphore_signal(
-                turn, inc=1, device_id=peer(hi, lo + 1), device_id_type=pl.DeviceIdType.MESH),
+                turn, inc=1, device_id=peer(hi, lo - 1), device_id_type=pl.DeviceIdType.MESH),
             "Q": lambda: pl.semaphore_wait(turn, 1),
         }
 
@@ -607,7 +612,7 @@
             pl.when(low)(lambda: among(names[:cut]))
             pl.when(jnp.logical_not(low))(lambda: among(names[cut:]))
 
-        pl.when(kind < KINDS.index("X"))(lambda: among(list(acts)))
+        among(list(acts))
         return carry
 
     def turns(a, carry):
@@ -617,9 +622,10 @@
             for at in range(1, len(words) // GROUP):
                 word = jnp.where(a == at, words[at * GROUP + r], word)
             near.append(word)
-        return lax.fori_loop(0, GROUP * many, functools.partial(run, near), carry)
-
-    lax.fori_loop(0, len(words) // GROUP, turns, 0)
+        left = jnp.minimum(GROUP * many, count - a * (GROUP * many))
+        return lax.fori_loop(0, left, functools.partial(run, near), carry)
+
+    lax.fori_loop(0, lax.div(count + (GROUP * many - 1), GROUP * many), turns, 0)
 
     def finish(j, carry):
         at = far_rows(j)

time: 115 us -> 111 us (0.965)
  the two profiles are of different devices: /device:TPU:9 before, /device:TPU:0 now
where the time goes in v6:
time: 111 us
  Pallas kernels  110 us (99%)
    pallas_call x1, Pallas kernels, per_device(): pl.pallas_call(functools.partial(kernel, n, cap, table), out_shape=pltpu....  110 us

profile of v6, /device:TPU:0, one launch (start us, length us, event | category | flops | bytes accessed | tf_op | source)
XLA Modules:
  0.0 110.6 jit_solution(2566776195494517628)
XLA Ops:
  0.0 109.6 %shard_map.73 = bf16[256,2048]{1,0:T(8,128)(2,1)S(1)} custom-call(bf16[256,2048]{1,0:T(8,128)(2,1)} %tok_ref.1, f32[1,2048]{1,0:T(1,128)} %bitcast.3, s32[2,256]{1,0:T(2,128)} %bitcast.4, f32[2,256]{1,0:T(2,128)} %bitcast.5, bf16[1,2048,1024]{2,1,0:T(8,128)(2,1)} %wg_ref.1, bf16[1,2048,1024]{2,1,0:T(8,128)(2,1)} %wu_ref.1, bf16[1,1024,2048]{2,1,0:T(8,128)(2,1)} %wd_ref.1), custom_call_target="tpu_custom_call" | custom-call | tf_op jit(solution)/shard_map/pallas_call | solution.py:669
  109.6 1.0 copy.9

commit v7 on v6

--- a/solution.py
+++ b/solution.py
@@ -16,49 +16,54 @@
 KINDS = "SZGTUVDEMFWNQ"
 COST = {"T": 1.6, "U": 2.05, "V": 2.05, "D": 1.96, "E": 1.96, "M": 1.84, "F": 1.7, "G": 0.15, "S": 0.1, "Z": 0.1}
 RANK = {"S": 0, "Z": 0, "G": 0.5, "T": 1, "N": -1, "M": 2, "F": 3, "D": 4, "E": 4, "U": 5, "V": 5}
-Z_BLOCK, Y_BLOCK, START, PACK, STEP, BACKLOG = 11.3, 5.6, 2.9, 3.8, 0.09, 3.0
-LAG = (2.2, 2.2, 2.2)
+Z_BLOCK, Y_BLOCK, START, PACK, STEP, BACKLOG = 11.4, 5.75, 2.9, 3.8, 0.09, 3.0
+LAG = (2.2, 2.2, 2.5)
 HANDOVER = 4
-PRIO = {(0, 0, 'E', 0): 0.8,
- (0, 0, 'M', 1): 5.6,
- (0, 1, 'D', 0): 4.8,
- (0, 1, 'T', 1): 5.1,
- (0, 1, 'T', 2): 4.6,
- (0, 1, 'V', 0): 0.3,
- (0, 1, 'V', 1): 1.0,
- (1, 0, 'E', 1): 4.9,
- (1, 0, 'G', 0): 2.1,
- (1, 0, 'M', 2): 5.8,
- (1, 0, 'M', 3): 0.2,
- (1, 0, 'S', 1): 4.2,
- (1, 0, 'T', 2): 0.7,
- (1, 0, 'U', 0): 6.0,
- (1, 0, 'V', 0): 2.9,
- (1, 1, 'E', 0): 0.5,
- (1, 1, 'E', 1): 6.0,
- (1, 1, 'E', 2): 0.4,
- (1, 1, 'E', 3): 2.6,
- (1, 1, 'G', 2): 1.1,
- (1, 1, 'G', 3): 2.6,
- (1, 1, 'S', 3): 2.3,
- (1, 1, 'T', 0): 2.6,
- (1, 1, 'T', 1): 5.9,
- (1, 1, 'T', 3): 4.9,
- (1, 1, 'Z', 0): 5.4}
-HOLD = {(0, 0, 'D', 0): 82,
- (0, 0, 'E', 0): 95,
- (0, 0, 'T', 2): 42,
- (0, 0, 'U', 3): 38,
- (0, 1, 'E', 0): 93,
- (1, 0, 'D', 1): 91,
- (1, 0, 'G', 2): 29,
+PRIO = {(0, 0, 'S', 1): 6.0,
+ (0, 0, 'T', 2): 5.3,
+ (0, 0, 'V', 1): 0.1,
+ (0, 1, 'E', 0): 5.5,
+ (0, 1, 'T', 1): 5.4,
+ (0, 1, 'T', 2): 5.3,
+ (0, 1, 'V', 0): 3.4,
+ (1, 0, 'D', 0): 2.0,
+ (1, 0, 'D', 1): 0.2,
+ (1, 0, 'D', 3): 2.4,
+ (1, 0, 'E', 3): 0.2,
+ (1, 0, 'M', 3): 4.0,
+ (1, 0, 'S', 0): 2.6,
+ (1, 0, 'T', 0): 4.7,
+ (1, 0, 'T', 2): 3.6,
+ (1, 0, 'U', 0): 2.4,
+ (1, 0, 'U', 2): 1.5,
+ (1, 0, 'V', 0): 2.4,
+ (1, 0, 'Z', 2): 1.3,
+ (1, 1, 'D', 0): 5.1,
+ (1, 1, 'D', 1): 0.1,
+ (1, 1, 'E', 0): 5.7,
+ (1, 1, 'E', 3): 0.3,
+ (1, 1, 'G', 0): 2.1,
+ (1, 1, 'M', 2): 0.1,
+ (1, 1, 'M', 3): 4.0,
+ (1, 1, 'S', 1): 4.8,
+ (1, 1, 'S', 3): 2.0,
+ (1, 1, 'T', 2): 3.6,
+ (1, 1, 'T', 3): 5.0,
+ (1, 1, 'Z', 0): 5.5}
+HOLD = {(0, 0, 'D', 0): 81,
+ (0, 0, 'E', 0): 84,
+ (0, 1, 'E', 0): 92,
+ (1, 0, 'E', 2): 80,
  (1, 0, 'S', 0): 27,
- (1, 0, 'T', 1): 36,
- (1, 0, 'U', 0): 69,
- (1, 0, 'V', 0): 69,
- (1, 1, 'E', 0): 64,
- (1, 1, 'E', 2): 64,
- (1, 1, 'T', 1): 65}
+ (1, 0, 'T', 1): 35,
+ (1, 0, 'U', 0): 57,
+ (1, 0, 'V', 0): 81,
+ (1, 1, 'E', 2): 80,
+ (1, 1, 'T', 1): 84,
+ (1, 1, 'T', 2): 49,
+ (1, 1, 'V', 1): 87,
+ (1, 1, 'V', 3): 47,
+ (1, 1, 'Z', 1): 64}
 
 
 def plan(zs):

time: 111 us -> 110 us (level)
  Pallas kernels: 110 us -> 108 us
    pallas_call x1, Pallas kernels: 110 us -> 108 us  [per_device(): pl.pallas_call(functools.partial(kernel, n, cap, table), out_shape=pltpu....]
where the time goes in v7:
time: 110 us; the launch traced here: 109 us
  Pallas kernels  108 us (98%)
    pallas_call x1, Pallas kernels, per_device(): pl.pallas_call(functools.partial(kernel, n, cap, table), out_shape=pltpu....  108 us

profile of v7, /device:TPU:0, one launch (start us, length us, event | category | flops | bytes accessed | tf_op | source)
XLA Modules:
  0.0 109.0 jit_solution(17642885085904191309)
XLA Ops:
  0.0 108.0 %shard_map.73 = bf16[256,2048]{1,0:T(8,128)(2,1)S(1)} custom-call(bf16[256,2048]{1,0:T(8,128)(2,1)} %tok_ref.1, f32[1,2048]{1,0:T(1,128)} %bitcast.3, s32[2,256]{1,0:T(2,128)} %bitcast.4, f32[2,256]{1,0:T(2,128)} %bitcast.5, bf16[1,2048,1024]{2,1,0:T(8,128)(2,1)} %wg_ref.1, bf16[1,2048,1024]{2,1,0:T(8,128)(2,1)} %wu_ref.1, bf16[1,1024,2048]{2,1,0:T(8,128)(2,1)} %wd_ref.1), custom_call_target="tpu_custom_call" | custom-call | tf_op jit(solution)/shard_map/pallas_call | solution.py:674
  108.0 1.0 copy.9

commit v8 on v7

--- a/solution.py
+++ b/solution.py
@@ -371,7 +371,7 @@
     for at in range(1, 2 * zs):
         count = jnp.where(where_am_i == at, len(table[at]), count)
 
-    step = 32
+    step = min(64, tok // PIECES)
 
     def norm(i, carry):
         at = pl.ds(pl.multiple_of(i * step, step), step)
@@ -452,7 +452,7 @@
             out_copy(j, dl, k).start()
         arrived[slot_rows(j, 0), dcol(k)] = got[:cap, :]
 
-    ftile = min(ff, 256)
+    ftile = min(ff, 512)
 
     def up(j, side):
         for which in (0, 1):

time: 110 us -> 109 us (level)
    pallas_call x1, Pallas kernels: 108 us -> 107 us  [per_device(): pl.pallas_call(functools.partial(kernel, n, cap, table), out_shape=pltpu....]
where the time goes in v8:
time: 109 us; the launch traced here: 108 us
  Pallas kernels  107 us (98%)
    pallas_call x1, Pallas kernels, per_device(): pl.pallas_call(functools.partial(kernel, n, cap, table), out_shape=pltpu....  107 us

profile of v8, /device:TPU:0, one launch (start us, length us, event | category | flops | bytes accessed | tf_op | source)
XLA Modules:
  0.0 107.6 jit_solution(2649836523644788935)
XLA Ops:
  0.0 106.6 %shard_map.73 = bf16[256,2048]{1,0:T(8,128)(2,1)S(1)} custom-call(bf16[256,2048]{1,0:T(8,128)(2,1)} %tok_ref.1, f32[1,2048]{1,0:T(1,128)} %bitcast.3, s32[2,256]{1,0:T(2,128)} %bitcast.4, f32[2,256]{1,0:T(2,128)} %bitcast.5, bf16[1,2048,1024]{2,1,0:T(8,128)(2,1)} %wg_ref.1, bf16[1,2048,1024]{2,1,0:T(8,128)(2,1)} %wu_ref.1, bf16[1,1024,2048]{2,1,0:T(8,128)(2,1)} %wd_ref.1), custom_call_target="tpu_custom_call" | custom-call | tf_op jit(solution)/shard_map/pallas_call | solution.py:674
  106.6 1.0 copy.9

commit v9 on v8

--- a/solution.py
+++ b/solution.py
@@ -11,8 +11,8 @@
 SUB = 4
 KD = 8
 KR = 8
-PIECES = 4
-GROUP = 8
+PIECES = 2
+GROUP = 4
 KINDS = "SZGTUVDEMFWNQ"
 COST = {"T": 1.6, "U": 2.05, "V": 2.05, "D": 1.96, "E": 1.96, "M": 1.84, "F": 1.7, "G": 0.15, "S": 0.1, "Z": 0.1}
 RANK = {"S": 0, "Z": 0, "G": 0.5, "T": 1, "N": -1, "M": 2, "F": 3, "D": 4, "E": 4, "U": 5, "V": 5}
@@ -371,7 +371,7 @@
     for at in range(1, 2 * zs):
         count = jnp.where(where_am_i == at, len(table[at]), count)
 
-    step = min(64, tok // PIECES)
+    step = min(128, tok // PIECES)
 
     def norm(i, carry):
         at = pl.ds(pl.multiple_of(i * step, step), step)

time: 109 us -> 108 us (level)
  no operation moved by 1% of the time
where the time goes in v9:
time: 108 us; the launch traced here: 107 us
  Pallas kernels  106 us (98%)
    pallas_call x1, Pallas kernels, per_device(): pl.pallas_call(functools.partial(kernel, n, cap, table), out_shape=pltpu....  106 us

profile of v9, /device:TPU:0, one launch (start us, length us, event | category | flops | bytes accessed | tf_op | source)
XLA Modules:
  0.0 107.4 jit_solution(12165276485640371350)
XLA Ops:
  0.0 106.4 %shard_map.73 = bf16[256,2048]{1,0:T(8,128)(2,1)S(1)} custom-call(bf16[256,2048]{1,0:T(8,128)(2,1)} %tok_ref.1, f32[1,2048]{1,0:T(1,128)} %bitcast.3, s32[2,256]{1,0:T(2,128)} %bitcast.4, f32[2,256]{1,0:T(2,128)} %bitcast.5, bf16[1,2048,1024]{2,1,0:T(8,128)(2,1)} %wg_ref.1, bf16[1,2048,1024]{2,1,0:T(8,128)(2,1)} %wu_ref.1, bf16[1,1024,2048]{2,1,0:T(8,128)(2,1)} %wd_ref.1), custom_call_target="tpu_custom_call" | custom-call | tf_op jit(solution)/shard_map/pallas_call | solution.py:674
  106.4 1.0 copy.9
